TPU v7x, 32 devices: a whole 2x2x4 slice. The times are simulated.
32 devices in a mesh: ep: 4 (over y, x), tp: 8 (over z, core).
Axes of the slice: x: 2, y: 2, z: 4, core: 2. Of those that a mesh axis runs over, the one named last changes fastest.
Arguments:
- tokens: bfloat16 [8192, 2048], P(('ep', 'tp')), may hold values from -6 to 6
- norm_gain: float32 [2048], replicated, may hold values from 0.1 to 1.9
- expert_ids: int32 [8192, 2], P(('ep', 'tp')), may hold values from 0 to 3, all different within a row; in each aligned block of 256 rows (0 to 255, 256 to 511, ...) at most 256 rows name the same one
- gate_weights: float32 [8192, 2], P(('ep', 'tp')), may hold values from 0.2 to 1
- w_gate: bfloat16 [4, 2048, 1024], P('ep', None, 'tp'), may hold values from -0.125 to 0.125
- w_up: bfloat16 [4, 2048, 1024], P('ep', None, 'tp'), may hold values from -0.125 to 0.125
- w_down: bfloat16 [4, 2048, 1024], P('ep', None, 'tp'), may hold values from -0.1875 to 0.1875
- dense_gate: bfloat16 [2048, 256], P('ep'), may hold values from -0.125 to 0.125
- dense_up: bfloat16 [2048, 256], P('ep'), may hold values from -0.125 to 0.125
- dense_down: bfloat16 [256, 2048], P(None, 'ep'), may hold values from -0.375 to 0.375
- mix_vector: float32 [2048], replicated, may hold values from -0.125 to 0.125
Outputs:
- mixed: bfloat16 [8192, 2048], P(('ep', 'tp'))
Inputs may be any that keep to these rules, and one draw needn't show every extreme that they name: `expert_ids`: A row names 2 different experts. In the rows of one device (aligned blocks of 256 rows) each expert is named by at most 256 rows, a bound that some block reaches.
All inputs are finite; a program needn't handle non-finite values.
Results may differ from a plain program's by a relative error of at most 0.0075.
Values may be sent and summed in bfloat16 or wider, within the bound.
A program may use at most 320 MiB of HBM per device.

v0:
```python
import functools

import jax
import jax.numpy as jnp
from jax import lax
from jax.experimental import pallas as pl
from jax.experimental.pallas import tpu as pltpu
from jax.sharding import PartitionSpec as P

MESH = pl.DeviceIdType.MESH
VMEM_BYTES = 65000 * 1024
CORES = 2
PIECES = 3
LANES = 128
eps = 1e-06


def moe_kernel(
    ne, nz, x_hbm, wg_hbm, wu_hbm, wd_hbm, dg_hbm, du_hbm, dd_hbm, ids_hbm, gates_hbm,
    gain_ref, mixv_ref, out_ref,
    xg, ws, dgs, dus, dds, acc, hbuf, ysend, yrecv, relay, side, ids, gates, mix_ref, stage, wts,
    lsem, wrecv, wright, wleft, wpartner, tsend, trecv, gsend, grecv, dsend, drecv, rsend, rrecv,
):
    me = lax.axis_index("ep")
    tp = lax.axis_index("tp")
    z = tp // CORES
    c = tp % CORES
    rows, width = xg.shape[1], xg.shape[2]
    peers = [(me + k) % ne for k in range(1, ne)]
    partner = z * CORES + (1 - c)

    local = [pltpu.make_async_copy(x_hbm, ysend.at[1], lsem.at[0])]
    for p, ref in enumerate((wg_hbm, wu_hbm, wd_hbm)):
        local.append(pltpu.make_async_copy(ref, ws.at[z, c, p], lsem.at[1 + p]))
    for p, (ref, slot) in enumerate(((dg_hbm, dgs), (du_hbm, dus), (dd_hbm, dds))):
        local.append(pltpu.make_async_copy(ref, slot.at[me], lsem.at[4 + p]))
    local.append(pltpu.make_async_copy(ids_hbm, ids, lsem.at[7]))
    local.append(pltpu.make_async_copy(gates_hbm, gates, lsem.at[8]))
    for copy in local:
        copy.start()

    barrier = pltpu.get_barrier_semaphore()
    for peer in peers:
        pl.semaphore_signal(barrier, inc=1, device_id={"ep": peer}, device_id_type=MESH)
    pl.semaphore_signal(barrier, inc=1, device_id={"tp": partner}, device_id_type=MESH)

    @pl.when(z > 0)
    def _():
        pl.semaphore_signal(barrier, inc=1, device_id={"tp": tp - CORES}, device_id_type=MESH)

    @pl.when(z < nz - 1)
    def _():
        pl.semaphore_signal(barrier, inc=1, device_id={"tp": tp + CORES}, device_id_type=MESH)

    neighbours = (z + nz - 1) // nz + (2 * nz - 2 - z) // nz
    pl.semaphore_wait(barrier, ne + neighbours)

    def weight_copy(src, p, target, sems):
        return pltpu.make_async_remote_copy(
            src_ref=ws.at[src, c, p], dst_ref=ws.at[src, c, p],
            send_sem=sems.at[src, p], recv_sem=wrecv.at[src, c, p],
            device_id={"tp": target}, device_id_type=MESH,
        )

    def to_right(src, p):
        return weight_copy(src, p, tp + CORES, wright)

    def to_left(src, p):
        return weight_copy(src, p, tp - CORES, wleft)

    def to_partner(src, p):
        return weight_copy(src, p, partner, wpartner)

    def await_piece(src, color, p):
        pltpu.make_async_remote_copy(
            src_ref=ws.at[src, color, p], dst_ref=ws.at[src, color, p],
            send_sem=wpartner.at[src, p], recv_sem=wrecv.at[src, color, p],
            device_id={"tp": partner}, device_id_type=MESH,
        ).wait_recv()

    def token_copy(k, block):
        return pltpu.make_async_remote_copy(
            src_ref=xg.at[block], dst_ref=xg.at[block],
            send_sem=tsend.at[k], recv_sem=trecv.at[block],
            device_id={"ep": peers[k]}, device_id_type=MESH,
        )

    def gate_copy(k, block):
        return pltpu.make_async_remote_copy(
            src_ref=wts.at[block], dst_ref=wts.at[block],
            send_sem=gsend.at[k], recv_sem=grecv.at[block],
            device_id={"ep": peers[k]}, device_id_type=MESH,
        )

    def dense_copy(k, p, block):
        slot = (dgs, dus, dds)[p]
        return pltpu.make_async_remote_copy(
            src_ref=slot.at[block], dst_ref=slot.at[block],
            send_sem=dsend.at[k, p], recv_sem=drecv.at[block, p],
            device_id={"ep": peers[k]}, device_id_type=MESH,
        )

    for p in range(PIECES):
        local[1 + p].wait()

        @pl.when(z < nz - 1)
        def _():
            to_right(z, p).start()

        @pl.when(z > 0)
        def _():
            to_left(z, p).start()

        to_partner(z, p).start()
    for i in (0, 7, 8):
        local[i].wait()
    tile = 32
    lane = lax.broadcasted_iota(jnp.int32, (tile, LANES), 1)

    def norm(i, carry):
        at = pl.ds(pl.multiple_of(i * tile, tile), tile)
        named, gate = ids[at, :], gates[at, :]
        weight = jnp.zeros((tile, LANES), jnp.float32)
        for k in range(named.shape[1]):
            weight += jnp.where(named[:, k : k + 1] == lane, gate[:, k : k + 1], 0.0)
        stage[at, :] = weight
        v = ysend[1, at, :].astype(jnp.float32)
        scale = lax.rsqrt(jnp.sum(v * v, axis=1, keepdims=True) * (1.0 / width) + eps)
        n = (v * scale * gain_ref[...]).astype(jnp.bfloat16)
        ysend[0, at, :] = n
        m = jnp.sum(n.astype(jnp.float32) * mixv_ref[...], axis=1, keepdims=True)
        mix_ref[at, :] = 1.0 / (1.0 + jnp.exp(-m))
        return carry

    lax.fori_loop(0, rows // tile, norm, 0)
    staged = [
        pltpu.make_async_copy(ysend.at[0], xg.at[me], lsem.at[9]),
        pltpu.make_async_copy(stage, wts.at[me], lsem.at[10]),
    ]
    for copy in staged:
        copy.start()
    for copy in staged:
        copy.wait()
    for k in range(ne - 1):
        token_copy(k, me).start()
    for k in range(ne - 1):
        gate_copy(k, me).start()

    def forward(d, p):
        @pl.when(z >= d)
        def _():
            await_piece(z - d, c, p)

            @pl.when(z < nz - 1)
            def _():
                to_right(z - d, p).start()

            to_partner(z - d, p).start()

        @pl.when(z + d < nz)
        def _():
            await_piece(z + d, c, p)

            @pl.when(z > 0)
            def _():
                to_left(z + d, p).start()

            to_partner(z + d, p).start()

    def hidden(src):
        await_piece(src, 1 - c, 0)
        await_piece(src, 1 - c, 1)

        def one(b, carry):
            x = xg[b]
            wg = jnp.concatenate([ws[src, i, 0] for i in range(CORES)], axis=1)
            g = jnp.dot(x, wg, preferred_element_type=jnp.float32)
            wu = jnp.concatenate([ws[src, i, 1] for i in range(CORES)], axis=1)
            u = jnp.dot(x, wu, preferred_element_type=jnp.float32)
            hbuf[src, b] = (g / (1.0 + jnp.exp(-g)) * u).astype(jnp.bfloat16)
            return carry

        lax.fori_loop(0, ne, one, 0)

    step = 512

    def down_block(src, b, first):
        h = hbuf[src, b]
        for j in range(0, width, step):
            w = jnp.concatenate([ws[src, i, 2, j : j + step, :] for i in range(CORES)], axis=1)
            y = lax.dot_general(
                h, w, (((1,), (1,)), ((), ())), preferred_element_type=jnp.float32
            )
            if first:
                acc[b, :, j : j + step] = y
            else:
                acc[b, :, j : j + step] += y

    def down(src, first):
        await_piece(src, 1 - c, 2)

        def one(b, carry):
            down_block(src, b, first)
            return carry

        lax.fori_loop(0, ne, one, 0)

    def both(d, fn):
        @pl.when(z >= d)
        def _():
            fn(z - d)

        @pl.when(z + d < nz)
        def _():
            fn(z + d)

    for p in range(PIECES):
        forward(1, p)
    for p in range(3):
        local[4 + p].wait()
    for k in range(ne - 1):
        token_copy(k, peers[k]).wait_recv()
    for k in range(ne - 1):
        gate_copy(k, peers[k]).wait_recv()
    for p in range(PIECES):
        for k in range(ne - 1):
            dense_copy(k, p, me).start()
    hidden(z)
    down(z, True)
    for d in range(2, nz):
        forward(d, 0)
        both(d - 1, hidden)
        forward(d, 1)
        both(d - 1, lambda src: down(src, False))
        if d == nz - 1:
            both(d, hidden)
        forward(d, 2)
        if d == 2:
            dense_side(ne, me, peers, dense_copy, xg, dgs, dus, dds, mix_ref, side)
    across, along, diagonal = me + 1 - 2 * (me % 2), (me + 2) % ne, ne - 1 - me
    half = rows // 2

    def back(k):
        block = (diagonal, diagonal, across, along, along, across)[k]
        peer = (across, along, across, along, along, across)[k]
        low = (0, half, 0, half, 0, half)[k]
        lands = relay.at[k] if k < 2 else yrecv.at[k % 2 if k < 4 else 1 - k % 2, low : low + half]
        return pltpu.make_async_remote_copy(
            src_ref=ysend.at[block, low : low + half], dst_ref=lands,
            send_sem=rsend.at[k], recv_sem=rrecv.at[k],
            device_id={"ep": peer}, device_id_type=MESH,
        )

    def column(block, at):
        return jnp.sum(jnp.where(lane == me, wts[block, at, :], 0.0), axis=1, keepdims=True)

    def fill(block, low, relayed):
        def one(i, carry):
            at = pl.ds(pl.multiple_of(low + i * tile, tile), tile)
            v = acc[block, at, :] * column(block, at)
            if relayed is not None:
                here = pl.ds(pl.multiple_of(i * tile, tile), tile)
                v += relay[relayed, here, :].astype(jnp.float32)
            ysend[block, at, :] = v.astype(jnp.bfloat16)
            return carry

        lax.fori_loop(0, half // tile, one, 0)

    both(nz - 1, lambda src: await_piece(src, 1 - c, 2))
    both(nz - 1, lambda src: down_block(src, diagonal, False))
    fill(diagonal, 0, None)
    back(0).start()
    fill(diagonal, half, None)
    back(1).start()
    both(nz - 1, lambda src: down_block(src, across, False))
    fill(across, 0, None)
    back(2).start()
    both(nz - 1, lambda src: down_block(src, along, False))
    fill(along, half, None)
    back(3).start()
    both(nz - 1, lambda src: down_block(src, me, False))
    back(0).wait_recv()
    fill(along, 0, 0)
    back(4).start()
    back(1).wait_recv()
    fill(across, half, 1)
    back(5).start()

    for k in range(ne - 1):
        token_copy(k, me).wait_send()
        gate_copy(k, me).wait_send()
        for p in range(PIECES):
            dense_copy(k, p, me).wait_send()

    for src in range(nz):
        for p in range(PIECES):
            @pl.when((z < nz - 1) & (z >= src))
            def _():
                to_right(src, p).wait_send()

            @pl.when((z > 0) & (z <= src))
            def _():
                to_left(src, p).wait_send()

            to_partner(src, p).wait_send()

    for k in range(6):
        back(k).wait_send()
    for k in range(2, 6):
        back(k).wait_recv()

    def combine(i, carry):
        at = pl.ds(pl.multiple_of(i * tile, tile), tile)
        total = side[at, :] + acc[me, at, :] * column(me, at)
        for k in range(2):
            total = total + yrecv[k, at, :].astype(jnp.float32)
        out_ref[at, :] = total.astype(jnp.bfloat16)
        return carry

    lax.fori_loop(0, rows // tile, combine, 0)


def dense_side(ne, me, peers, dense_copy, xg, dgs, dus, dds, mix_ref, side):
    for k in range(ne - 1):
        for p in range(PIECES):
            dense_copy(k, p, peers[k]).wait_recv()
    deep, wide = dgs.shape[1], dds.shape[2]
    g = u = None
    for e in range(ne):
        x = xg[me, :, e * deep : (e + 1) * deep]
        ge = jnp.dot(x, dgs[e], preferred_element_type=jnp.float32)
        ue = jnp.dot(x, dus[e], preferred_element_type=jnp.float32)
        g, u = (ge, ue) if e == 0 else (g + ge, u + ue)
    h = (g / (1.0 + jnp.exp(-g)) * u).astype(jnp.bfloat16)
    for e in range(ne):
        o = jnp.dot(h, dds[e], preferred_element_type=jnp.float32)
        side[:, e * wide : (e + 1) * wide] = mix_ref[...] * o


def fused_layer(
    ne, tp, tokens, norm_gain, expert_ids, gate_weights,
    w_gate, w_up, w_down, dense_gate, dense_up, dense_down, mix_vector,
):
    nz = tp // CORES
    rows, width = tokens.shape
    topk = expert_ids.shape[1]
    shard = w_gate.shape[2]
    bf, f32 = jnp.bfloat16, jnp.float32
    dma = pltpu.SemaphoreType.DMA
    hbm = pl.BlockSpec(memory_space=pl.ANY)
    vmem = pl.BlockSpec(memory_space=pltpu.VMEM)
    flops = 6 * ne * rows * width * shard * tp
    return pl.pallas_call(
        functools.partial(moe_kernel, ne, nz),
        out_shape=jax.ShapeDtypeStruct((rows, width), bf),
        in_specs=[hbm] * 9 + [vmem] * 2,
        out_specs=vmem,
        scratch_shapes=[
            pltpu.VMEM((ne, rows, width), bf),
            pltpu.VMEM((nz, CORES, PIECES, width, shard), bf),
            pltpu.VMEM((ne,) + dense_gate.shape, bf),
            pltpu.VMEM((ne,) + dense_up.shape, bf),
            pltpu.VMEM((ne,) + dense_down.shape, bf),
            pltpu.VMEM((ne, rows, width), f32),
            pltpu.VMEM((nz, ne, rows, CORES * shard), bf),
            pltpu.VMEM((ne, rows, width), bf),
            pltpu.VMEM((2, rows, width), bf),
            pltpu.VMEM((2, rows // 2, width), bf),
            pltpu.VMEM((rows, width), f32),
            pltpu.VMEM((rows, topk), jnp.int32),
            pltpu.VMEM((rows, topk), f32),
            pltpu.VMEM((rows, 1), f32),
            pltpu.VMEM((rows, LANES), f32),
            pltpu.VMEM((ne, rows, LANES), f32),
            dma((11,)),
            dma((nz, CORES, PIECES)),
            dma((nz, PIECES)),
            dma((nz, PIECES)),
            dma((nz, PIECES)),
            dma((ne,)),
            dma((ne,)),
            dma((ne,)),
            dma((ne,)),
            dma((ne, PIECES)),
            dma((ne, PIECES)),
            dma((6,)),
            dma((6,)),
        ],
        compiler_params=pltpu.CompilerParams(
            collective_id=0, has_side_effects=True, vmem_limit_bytes=VMEM_BYTES
        ),
        cost_estimate=pl.CostEstimate(
            flops=flops, bytes_accessed=8 * rows * width, transcendentals=ne * rows * shard * tp
        ),
    )(
        tokens, w_gate[0], w_up[0], w_down[0], dense_gate, dense_up, dense_down,
        expert_ids, gate_weights, norm_gain.reshape(1, width), mix_vector.reshape(1, width),
    )


def fits(ne, tp, tokens, w_gate, dense_gate):
    rows, width = tokens.shape
    shard = w_gate.shape[2]
    block = rows * width
    size = 2 * ne * block * 5 + 8 * block + 2 * PIECES * width * shard * tp
    size += 2 * ne * rows * shard * tp + 6 * ne * dense_gate.size
    aligned = shard % 128 == 0 and width % 512 == 0 and rows % 64 == 0
    return ne == 4 and tp % CORES == 0 and tp > 2 * CORES and aligned and size < VMEM_BYTES * 15 // 16


def dense_branch(normed, dense_gate, dense_up, dense_down, mix_vector):
    dense_g = jnp.dot(
        normed,
        lax.all_gather(dense_gate, "ep", axis=0, tiled=True),
        preferred_element_type=jnp.float32,
    )
    dense_u = jnp.dot(
        normed,
        lax.all_gather(dense_up, "ep", axis=0, tiled=True),
        preferred_element_type=jnp.float32,
    )
    dense_hidden = (jax.nn.silu(dense_g) * dense_u).astype(jnp.bfloat16)
    dense_out = jnp.dot(
        dense_hidden,
        lax.all_gather(dense_down, "ep", axis=1, tiled=True),
        preferred_element_type=jnp.float32,
    )
    mix = jax.nn.sigmoid(jnp.sum(normed.astype(jnp.float32) * mix_vector, axis=1))
    return mix[:, None] * dense_out


def on_device(
    tokens,
    norm_gain,
    expert_ids,
    gate_weights,
    w_gate,
    w_up,
    w_down,
    dense_gate,
    dense_up,
    dense_down,
    mix_vector,
):
    groups = lax.axis_size("ep")
    ring = lax.axis_size("tp")
    if fits(groups, ring, tokens, w_gate, dense_gate):
        return fused_layer(
            groups, ring, tokens, norm_gain, expert_ids, gate_weights,
            w_gate, w_up, w_down, dense_gate, dense_up, dense_down, mix_vector,
        )
    values = tokens.astype(jnp.float32)
    scale = lax.rsqrt(jnp.mean(values * values, axis=1, keepdims=True) + eps)
    normed = (values * scale * norm_gain).astype(jnp.bfloat16)
    count_tok, topk = expert_ids.shape
    width = tokens.shape[1]
    capacity = 2 * count_tok * topk // groups
    flat_ids = expert_ids.reshape(-1)
    onehot = (flat_ids[:, None] == jnp.arange(groups, dtype=jnp.int32)[None, :]).astype(jnp.int32)
    before = jnp.cumsum(onehot, axis=0) - onehot
    slot = jnp.sum(before * onehot, axis=1)
    dest = flat_ids * capacity + slot
    owner = jnp.arange(count_tok * topk, dtype=jnp.int32) // topk
    buffer = jnp.zeros((groups * capacity, width), jnp.bfloat16).at[dest].set(normed[owner])
    arrived = lax.all_to_all(
        buffer.reshape(groups, capacity, width), "ep", split_axis=0, concat_axis=0, tiled=True
    )
    rows = arrived.reshape(groups * capacity, width)
    gate = jnp.dot(
        rows,
        lax.all_gather(w_gate, "tp", axis=2, tiled=True)[0],
        preferred_element_type=jnp.float32,
    )
    upper = jnp.dot(
        rows, lax.all_gather(w_up, "tp", axis=2, tiled=True)[0], preferred_element_type=jnp.float32
    )
    hidden_all = (jax.nn.silu(gate) * upper).astype(jnp.bfloat16)
    expert_out = lax.dot_general(
        hidden_all,
        lax.all_gather(w_down, "tp", axis=2, tiled=True)[0],
        (((1,), (1,)), ((), ())),
        preferred_element_type=jnp.float32,
    )
    results = expert_out.astype(jnp.bfloat16).reshape(groups, capacity, width)
    returned = lax.all_to_all(results, "ep", split_axis=0, concat_axis=0, tiled=True)
    picked = returned.reshape(groups * capacity, width)[dest].reshape(count_tok, topk, width)
    routed = jnp.einsum("tk,tkd->td", gate_weights, picked.astype(jnp.float32))
    side = dense_branch(normed, dense_gate, dense_up, dense_down, mix_vector)
    return (routed + side).astype(jnp.bfloat16)


def solution(mesh):
    placed = (
        P(("ep", "tp"), None),
        P(),
        P(("ep", "tp"), None),
        P(("ep", "tp"), None),
        P("ep", None, "tp"),
        P("ep", None, "tp"),
        P("ep", None, "tp"),
        P("ep", None),
        P("ep", None),
        P(None, "ep"),
        P(),
    )
    return jax.shard_map(
        on_device, mesh=mesh, in_specs=placed, out_specs=P(("ep", "tp"), None), check_vma=False
    )
```

profile of v0, /device:TPU:0, one launch (start us, length us, event | category | flops | bytes accessed | tf_op | source)
XLA Modules:
  0.0 152.3 jit_solution(301374735613548810)
XLA Ops:
  0.0 0.0 copy-start
  0.0 0.7 copy-done
  0.7 0.0 copy-start.1
  0.7 0.8 copy.12.ids_hbm
  1.5 0.0 copy-done.1
  1.5 0.8 copy.13.gates_hbm
  2.3 147.8 %shard_map.109 = bf16[256,2048]{1,0:T(8,128)(2,1)} custom-call(bf16[256,2048]{1,0:T(8,128)(2,1)} %x_hbm.1, bf16[2048,128]{1,0:T(8,128)(2,1)} %bitcast.5, bf16[2048,128]{1,0:T(8,128)(2,1)} %bitcast.6, bf16[2048,128]{1,0:T(8,128)(2,1)} %bitcast.7, bf16[512,256]{1,0:T(8,128)(2,1)} %dg_hbm.1, bf16[512,256]{1,0:T(8,128)(2,1)} %du_hbm.1, bf16[256,512]{1,0:T(8,128)(2,1)} %dd_hbm.1, ...), custom_call_target="tpu_custom_call" | custom-call | flops 12884901888 | bytes 4194304 | tf_op jit(solution)/shard_map/pallas_call | solution.py:353
  150.0 2.3 %copy.15 = bf16[256,2048]{1,0:T(8,128)(2,1)} copy(bf16[256,2048]{1,0:T(8,128)(2,1)} %shard_map.109) | data formatting | bytes 2097152
Async XLA Ops:
  0.0 0.7 copy-start
  0.7 0.8 copy-start.1
where the time goes:
time: 153 us; the launch traced here: 152 us
  Pallas kernels  148 us (97%)
  local copies, waits for them, and re-layouts  4.58 us (3%)
    pallas_call x1, Pallas kernels, fused_layer(): pl.pallas_call(functools.partial(moe_kernel, ne, nz), out_shape=jax.Shape...  148 us
    unnamed x7, local copies, waits for them, and re-layouts  4.58 us

commit v1 on v0

v1 whole, which is shorter than its diff:
```python
import functools

import jax
import jax.numpy as jnp
from jax import lax
from jax.experimental import pallas as pl
from jax.experimental.pallas import tpu as pltpu
from jax.sharding import PartitionSpec as P

MESH = pl.DeviceIdType.MESH
VMEM_BYTES = 65000 * 1024
CORES = 2
CHUNK = 256
SUB = 8
eps = 1e-06


def moe_kernel(
    ne, nz, x_hbm, wg_hbm, wu_hbm, wd_hbm, dg_hbm, du_hbm, dd_hbm, ids_ref, gates_ref,
    gain_ref, mixv_ref, out_ref,
    xin, xg, ws, wd, dgs, dus, dds, hbuf, own, keep, ysend, yrecv, relay, side, mix_ref, wts, wcol,
    lsem, wrecv, wright, wleft, wpartner, crecv, cright, cleft, cpartner,
    tsend, trecv, gsend, grecv, dsend, drecv, psend, precv, rsend, rrecv,
):
    me = lax.axis_index("ep")
    tp = lax.axis_index("tp")
    z = tp // CORES
    c = tp % CORES
    rows, width = xg.shape[1], xg.shape[2]
    nj, cw = ysend.shape[0], ysend.shape[3]
    half = rows // 2
    shard = ws.shape[4]
    across, along, diagonal = me + 1 - 2 * (me % 2), (me + 2) % ne, ne - 1 - me
    peers = [across, along, diagonal]
    partner = z * CORES + (1 - c)
    inner = (z > 0) & (z < nz - 1)

    local = [pltpu.make_async_copy(wg_hbm, ws.at[z, c, 0], lsem.at[0])]
    local.append(pltpu.make_async_copy(wu_hbm, ws.at[z, c, 1], lsem.at[1]))
    local.append(pltpu.make_async_copy(x_hbm, xin, lsem.at[2]))
    local.append(pltpu.make_async_copy(wd_hbm, wd.at[z, c], lsem.at[3]))
    for p, (ref, slot) in enumerate(((dg_hbm, dgs), (du_hbm, dus), (dd_hbm, dds))):
        local.append(pltpu.make_async_copy(ref, slot.at[me], lsem.at[4 + p]))
    for copy in local:
        copy.start()

    barrier = pltpu.get_barrier_semaphore()
    for peer in peers:
        pl.semaphore_signal(barrier, inc=1, device_id={"ep": peer}, device_id_type=MESH)
    pl.semaphore_signal(barrier, inc=1, device_id={"tp": partner}, device_id_type=MESH)

    @pl.when(z > 0)
    def _():
        pl.semaphore_signal(barrier, inc=1, device_id={"tp": tp - CORES}, device_id_type=MESH)

    @pl.when(z < nz - 1)
    def _():
        pl.semaphore_signal(barrier, inc=1, device_id={"tp": tp + CORES}, device_id_type=MESH)

    neighbours = (z + nz - 1) // nz + (2 * nz - 2 - z) // nz
    pl.semaphore_wait(barrier, ne + neighbours)

    def remote(src, dst, send, recv, **device):
        return pltpu.make_async_remote_copy(
            src_ref=src, dst_ref=dst, send_sem=send, recv_sem=recv,
            device_id=device, device_id_type=MESH,
        )

    def weight_copy(src, p, target, sems):
        piece = ws.at[src, c, p]
        return remote(piece, piece, sems.at[src, p], wrecv.at[src, c, p], tp=target)

    def to_right(src, p):
        return weight_copy(src, p, tp + CORES, wright)

    def to_left(src, p):
        return weight_copy(src, p, tp - CORES, wleft)

    def to_partner(src, p):
        return weight_copy(src, p, partner, wpartner)

    def await_piece(src, color, p):
        piece = ws.at[src, color, p]
        remote(piece, piece, wpartner.at[src, p], wrecv.at[src, color, p], tp=partner).wait_recv()

    def chunk(j):
        return pl.ds(pl.multiple_of(j * cw, cw), cw)

    def chunk_copy(src, j, target, sems):
        piece = wd.at[src, c, chunk(j)]
        return remote(piece, piece, sems.at[src], crecv.at[j, src, c], tp=target)

    def c_right(src, j):
        chunk_copy(src, j, tp + CORES, cright).start()

    def c_left(src, j):
        chunk_copy(src, j, tp - CORES, cleft).start()

    def c_partner(src, j):
        chunk_copy(src, j, partner, cpartner).start()

    def await_chunk(src, color, j):
        piece = wd.at[src, color, chunk(j)]
        remote(piece, piece, cpartner.at[src], crecv.at[j, src, color], tp=partner).wait_recv()

    def await_sent(src, sems):
        piece = wd.at[src, c]
        remote(piece, piece, sems.at[src], crecv.at[0, src, c], tp=partner).wait_send()

    def token_copy(k):
        block = (me, me, across, along)[k]
        peer = (across, along, along, across)[k]
        low, size = ((0, rows), (0, rows), (0, half), (half, half))[k]
        piece = xg.at[block, low : low + size]
        return remote(piece, piece, tsend.at[k], trecv.at[k], ep=peer)

    def await_token(k):
        block = (across, along, diagonal, diagonal)[k]
        low, size = ((0, rows), (0, rows), (0, half), (half, half))[k]
        piece = xg.at[block, low : low + size]
        remote(piece, piece, tsend.at[k], trecv.at[k], ep=across).wait_recv()

    def gate_copy(k, block):
        return remote(wts.at[block], wts.at[block], gsend.at[k], grecv.at[block], ep=peers[k])

    def dense_piece(p, block, color):
        slot = (dgs, dus, dds)[p]
        part = slot.shape[1] // CORES
        return slot.at[block, pl.ds(pl.multiple_of(color * part, part), part)]

    def dense_copy(k, p, block):
        piece = dense_piece(p, block, c)
        return remote(piece, piece, dsend.at[k, p], drecv.at[block, p], ep=peers[k])

    def dense_partner(k, p, color):
        piece = dense_piece(p, peers[k], color)
        return remote(piece, piece, psend.at[k, p], precv.at[k, p], tp=partner)

    for p in range(2):
        local[p].wait()

        @pl.when(z < nz - 1)
        def _():
            to_right(z, p).start()

        @pl.when(z > 0)
        def _():
            to_left(z, p).start()

        to_partner(z, p).start()
    local[2].wait()

    expert = lax.broadcasted_iota(jnp.int32, (SUB, rows), 0)
    named, gate = ids_ref[...], gates_ref[...]
    weight = jnp.zeros((SUB, rows), jnp.float32)
    for k in range(ids_ref.shape[0]):
        weight += jnp.where(named[k : k + 1, :] == expert, gate[k : k + 1, :], 0.0)
    wts[me] = weight
    tile = 32

    def norm(i, carry):
        at = pl.ds(pl.multiple_of(i * tile, tile), tile)
        v = xin[at, :].astype(jnp.float32)
        scale = lax.rsqrt(jnp.sum(v * v, axis=1, keepdims=True) * (1.0 / width) + eps)
        n = (v * scale * gain_ref[...]).astype(jnp.bfloat16)
        xg[me, at, :] = n
        m = jnp.sum(n.astype(jnp.float32) * mixv_ref[...], axis=1, keepdims=True)
        mix_ref[at, :] = 1.0 / (1.0 + jnp.exp(-m))
        return carry

    lax.fori_loop(0, rows // tile, norm, 0)
    local[3].wait()

    def own_chunks(j, carry):
        c_partner(z, j)

        @pl.when(z == 0)
        def _():
            c_right(z, j)

        @pl.when(z == nz - 1)
        def _():
            c_left(z, j)

        return carry

    lax.fori_loop(0, nj, own_chunks, 0)
    for k in range(2):
        token_copy(k).start()
    for k in range(ne - 1):
        gate_copy(k, me).start()
    for p in range(3):
        local[4 + p].wait()
    for p in range(3):
        for k in range(ne - 1):
            dense_copy(k, p, me).start()

    def forward(d, p):
        @pl.when(z >= d)
        def _():
            await_piece(z - d, c, p)

            @pl.when(z < nz - 1)
            def _():
                to_right(z - d, p).start()

            to_partner(z - d, p).start()

        @pl.when(z + d < nz)
        def _():
            await_piece(z + d, c, p)

            @pl.when(z > 0)
            def _():
                to_left(z + d, p).start()

            to_partner(z + d, p).start()

    def hidden(src):
        await_piece(src, 1 - c, 0)
        await_piece(src, 1 - c, 1)
        at = pl.ds(pl.multiple_of(src * (CORES * shard), CORES * shard), CORES * shard)

        def one(b, carry):
            x = xg[b]
            wg = jnp.concatenate([ws[src, i, 0] for i in range(CORES)], axis=1)
            g = jnp.dot(x, wg, preferred_element_type=jnp.float32)
            wu = jnp.concatenate([ws[src, i, 1] for i in range(CORES)], axis=1)
            u = jnp.dot(x, wu, preferred_element_type=jnp.float32)
            hbuf[b, :, at] = (g / (1.0 + jnp.exp(-g)) * u * wcol[b]).astype(jnp.bfloat16)
            return carry

        lax.fori_loop(0, ne, one, 0)

    def both(d, fn):
        @pl.when(z >= d)
        def _():
            fn(z - d)

        @pl.when(z + d < nz)
        def _():
            fn(z + d)

    def own_chunk(j):
        @pl.when(inner)
        def _():
            c_right(z, j)
            c_left(z, j)

    for p in range(2):
        forward(1, p)
    for k in range(2):
        await_token(k)
        token_copy(2 + k).start()
    for d in range(2, nz - 1):
        for p in range(2):
            forward(d, p)
    for j in range(2):
        own_chunk(j)
    for k in range(ne - 1):
        gate_copy(k, peers[k]).wait_recv()
    lane = lax.broadcasted_iota(jnp.int32, (rows, SUB), 1)
    for b in range(ne):
        column = jnp.where(lane == me, wts[b].T, 0.0)
        wcol[b] = jnp.sum(column, axis=1, keepdims=True)
    for k in range(2, 4):
        await_token(k)
    hidden(z)
    for d in range(1, nz - 1):
        both(d, hidden)
    for k in range(ne - 1):
        for p in range(3):
            dense_copy(k, p, peers[k]).wait_recv()
            dense_partner(k, p, c).start()
    forward(nz - 1, 0)
    for k in range(ne - 1):
        for p in range(3):
            dense_partner(k, p, 1 - c).wait_recv()
    dense_side(ne, me, xg, dgs, dus, dds, mix_ref, side)
    forward(nz - 1, 1)
    both(nz - 1, hidden)

    def back(k, j):
        block = (diagonal, diagonal, across, along, along, across)[k]
        peer = (across, along, across, along, along, across)[k]
        low = (0, half, 0, half, 0, half)[k]
        spot = (0, 1, 0, 1, 1, 0)[k]
        lands = relay.at[j, k] if k < 2 else yrecv.at[j, spot, low : low + half]
        return remote(
            ysend.at[j, block, low : low + half], lands, rsend.at[k], rrecv.at[j, k], ep=peer
        )

    def await_back(k):
        piece = relay.at[:, 0]
        remote(piece, piece, rsend.at[k], rrecv.at[0, k], ep=across).wait_send()

    def take(j):
        @pl.when(j + 2 < nj)
        def _():
            own_chunk(j + 2)

        for d in range(1, nz):
            @pl.when(z >= d)
            def _():
                await_chunk(z - d, c, j)

                @pl.when(z < nz - 1)
                def _():
                    c_right(z - d, j)

                c_partner(z - d, j)

            @pl.when(z + d < nz)
            def _():
                await_chunk(z + d, c, j)

                @pl.when(z > 0)
                def _():
                    c_left(z + d, j)

                c_partner(z + d, j)

        for src in range(nz):
            await_chunk(src, 1 - c, j)

    def produce(j):
        at = chunk(j)
        w = jnp.concatenate([wd[s, i, at, :] for s in range(nz) for i in range(CORES)], axis=1)

        def rows_of(b):
            return lax.dot_general(
                hbuf[b], w, (((1,), (1,)), ((), ())), preferred_element_type=jnp.float32
            )

        ysend[j, diagonal] = rows_of(diagonal).astype(jnp.bfloat16)
        back(0, j).start()
        back(1, j).start()
        y = rows_of(across)
        ysend[j, across, :half] = y[:half].astype(jnp.bfloat16)
        keep[j, 1] = y[half:]
        back(2, j).start()
        y = rows_of(along)
        ysend[j, along, half:] = y[half:].astype(jnp.bfloat16)
        keep[j, 0] = y[:half]
        back(3, j).start()
        own[:, at] = rows_of(me)

    def pass_on(j):
        back(0, j).wait_recv()
        v = keep[j, 0] + relay[j, 0].astype(jnp.float32)
        ysend[j, along, :half] = v.astype(jnp.bfloat16)
        back(4, j).start()
        back(1, j).wait_recv()
        v = keep[j, 1] + relay[j, 1].astype(jnp.float32)
        ysend[j, across, half:] = v.astype(jnp.bfloat16)
        back(5, j).start()

    def combine(j):
        for k in range(2, 6):
            back(k, j).wait_recv()
        at = chunk(j)
        total = side[:, at] + own[:, at]
        for k in range(2):
            total = total + yrecv[j, k].astype(jnp.float32)
        out_ref[:, at] = total.astype(jnp.bfloat16)

    def step(j, carry):
        take(j)
        produce(j)

        @pl.when(j >= 1)
        def _():
            pass_on(j - 1)

        @pl.when(j >= 2)
        def _():
            combine(j - 2)

        return carry

    lax.fori_loop(0, nj, step, 0)
    pass_on(nj - 1)
    combine(nj - 2)
    combine(nj - 1)

    for k in range(4):
        token_copy(k).wait_send()
    for k in range(ne - 1):
        gate_copy(k, me).wait_send()
        for p in range(3):
            dense_copy(k, p, me).wait_send()
            dense_partner(k, p, c).wait_send()
    for src in range(nz):
        @pl.when((z < nz - 1) & (z >= src))
        def _():
            for p in range(2):
                to_right(src, p).wait_send()
            await_sent(src, cright)

        @pl.when((z > 0) & (z <= src))
        def _():
            for p in range(2):
                to_left(src, p).wait_send()
            await_sent(src, cleft)

        for p in range(2):
            to_partner(src, p).wait_send()
        await_sent(src, cpartner)
    for k in range(6):
        await_back(k)


def dense_side(ne, me, xg, dgs, dus, dds, mix_ref, side):
    deep, wide = dgs.shape[1], dds.shape[2]
    g = u = None
    for e in range(ne):
        x = xg[me, :, e * deep : (e + 1) * deep]
        ge = jnp.dot(x, dgs[e], preferred_element_type=jnp.float32)
        ue = jnp.dot(x, dus[e], preferred_element_type=jnp.float32)
        g, u = (ge, ue) if e == 0 else (g + ge, u + ue)
    h = (g / (1.0 + jnp.exp(-g)) * u).astype(jnp.bfloat16)
    for e in range(ne):
        o = jnp.dot(h, dds[e], preferred_element_type=jnp.float32)
        side[:, e * wide : (e + 1) * wide] = mix_ref[...] * o


def fused_layer(
    ne, tp, tokens, norm_gain, expert_ids, gate_weights,
    w_gate, w_up, w_down, dense_gate, dense_up, dense_down, mix_vector,
):
    nz = tp // CORES
    rows, width = tokens.shape
    shard = w_gate.shape[2]
    nj = width // CHUNK
    half = rows // 2
    bf, f32 = jnp.bfloat16, jnp.float32
    dma = pltpu.SemaphoreType.DMA
    hbm = pl.BlockSpec(memory_space=pl.ANY)
    vmem = pl.BlockSpec(memory_space=pltpu.VMEM)
    flops = 6 * ne * rows * width * shard * tp
    return pl.pallas_call(
        functools.partial(moe_kernel, ne, nz),
        out_shape=jax.ShapeDtypeStruct((rows, width), bf),
        in_specs=[hbm] * 7 + [vmem] * 4,
        out_specs=vmem,
        scratch_shapes=[
            pltpu.VMEM((rows, width), bf),
            pltpu.VMEM((ne, rows, width), bf),
            pltpu.VMEM((nz, CORES, 2, width, shard), bf),
            pltpu.VMEM((nz, CORES, width, shard), bf),
            pltpu.VMEM((ne,) + dense_gate.shape, bf),
            pltpu.VMEM((ne,) + dense_up.shape, bf),
            pltpu.VMEM((ne,) + dense_down.shape, bf),
            pltpu.VMEM((ne, rows, tp * shard), bf),
            pltpu.VMEM((rows, width), f32),
            pltpu.VMEM((nj, 2, half, CHUNK), f32),
            pltpu.VMEM((nj, ne, rows, CHUNK), bf),
            pltpu.VMEM((nj, 2, rows, CHUNK), bf),
            pltpu.VMEM((nj, 2, half, CHUNK), bf),
            pltpu.VMEM((rows, width), f32),
            pltpu.VMEM((rows, 1), f32),
            pltpu.VMEM((ne, SUB, rows), f32),
            pltpu.VMEM((ne, rows, 1), f32),
            dma((7,)),
            dma((nz, CORES, 2)),
            dma((nz, 2)),
            dma((nz, 2)),
            dma((nz, 2)),
            dma((nj, nz, CORES)),
            dma((nz,)),
            dma((nz,)),
            dma((nz,)),
            dma((4,)),
            dma((4,)),
            dma((ne,)),
            dma((ne,)),
            dma((ne, 3)),
            dma((ne, 3)),
            dma((ne, 3)),
            dma((ne, 3)),
            dma((6,)),
            dma((nj, 6)),
        ],
        compiler_params=pltpu.CompilerParams(
            collective_id=0, has_side_effects=True, vmem_limit_bytes=VMEM_BYTES
        ),
        cost_estimate=pl.CostEstimate(
            flops=flops, bytes_accessed=8 * rows * width, transcendentals=ne * rows * shard * tp
        ),
    )(
        tokens, w_gate[0], w_up[0], w_down[0], dense_gate, dense_up, dense_down,
        expert_ids.T, gate_weights.T, norm_gain.reshape(1, width), mix_vector.reshape(1, width),
    )


def fits(ne, tp, tokens, w_gate, dense_gate):
    rows, width = tokens.shape
    shard = w_gate.shape[2]
    block = rows * width
    size = 2 * ne * block * 2 + 24 * block + 6 * width * shard * tp
    size += 2 * ne * rows * shard * tp + 6 * ne * dense_gate.size + 1024 * ne * rows
    aligned = shard % 128 == 0 and width % (2 * CHUNK) == 0 and rows % 64 == 0
    return ne == 4 and tp % CORES == 0 and tp > 2 * CORES and aligned and size < VMEM_BYTES * 15 // 16


def dense_branch(normed, dense_gate, dense_up, dense_down, mix_vector):
    dense_g = jnp.dot(
        normed,
        lax.all_gather(dense_gate, "ep", axis=0, tiled=True),
        preferred_element_type=jnp.float32,
    )
    dense_u = jnp.dot(
        normed,
        lax.all_gather(dense_up, "ep", axis=0, tiled=True),
        preferred_element_type=jnp.float32,
    )
    dense_hidden = (jax.nn.silu(dense_g) * dense_u).astype(jnp.bfloat16)
    dense_out = jnp.dot(
        dense_hidden,
        lax.all_gather(dense_down, "ep", axis=1, tiled=True),
        preferred_element_type=jnp.float32,
    )
    mix = jax.nn.sigmoid(jnp.sum(normed.astype(jnp.float32) * mix_vector, axis=1))
    return mix[:, None] * dense_out


def on_device(
    tokens,
    norm_gain,
    expert_ids,
    gate_weights,
    w_gate,
    w_up,
    w_down,
    dense_gate,
    dense_up,
    dense_down,
    mix_vector,
):
    groups = lax.axis_size("ep")
    ring = lax.axis_size("tp")
    if fits(groups, ring, tokens, w_gate, dense_gate):
        return fused_layer(
            groups, ring, tokens, norm_gain, expert_ids, gate_weights,
            w_gate, w_up, w_down, dense_gate, dense_up, dense_down, mix_vector,
        )
    values = tokens.astype(jnp.float32)
    scale = lax.rsqrt(jnp.mean(values * values, axis=1, keepdims=True) + eps)
    normed = (values * scale * norm_gain).astype(jnp.bfloat16)
    count_tok, topk = expert_ids.shape
    width = tokens.shape[1]
    capacity = 2 * count_tok * topk // groups
    flat_ids = expert_ids.reshape(-1)
    onehot = (flat_ids[:, None] == jnp.arange(groups, dtype=jnp.int32)[None, :]).astype(jnp.int32)
    before = jnp.cumsum(onehot, axis=0) - onehot
    slot = jnp.sum(before * onehot, axis=1)
    dest = flat_ids * capacity + slot
    owner = jnp.arange(count_tok * topk, dtype=jnp.int32) // topk
    buffer = jnp.zeros((groups * capacity, width), jnp.bfloat16).at[dest].set(normed[owner])
    arrived = lax.all_to_all(
        buffer.reshape(groups, capacity, width), "ep", split_axis=0, concat_axis=0, tiled=True
    )
    rows = arrived.reshape(groups * capacity, width)
    gate = jnp.dot(
        rows,
        lax.all_gather(w_gate, "tp", axis=2, tiled=True)[0],
        preferred_element_type=jnp.float32,
    )
    upper = jnp.dot(
        rows, lax.all_gather(w_up, "tp", axis=2, tiled=True)[0], preferred_element_type=jnp.float32
    )
    hidden_all = (jax.nn.silu(gate) * upper).astype(jnp.bfloat16)
    expert_out = lax.dot_general(
        hidden_all,
        lax.all_gather(w_down, "tp", axis=2, tiled=True)[0],
        (((1,), (1,)), ((), ())),
        preferred_element_type=jnp.float32,
    )
    results = expert_out.astype(jnp.bfloat16).reshape(groups, capacity, width)
    returned = lax.all_to_all(results, "ep", split_axis=0, concat_axis=0, tiled=True)
    picked = returned.reshape(groups * capacity, width)[dest].reshape(count_tok, topk, width)
    routed = jnp.einsum("tk,tkd->td", gate_weights, picked.astype(jnp.float32))
    side = dense_branch(normed, dense_gate, dense_up, dense_down, mix_vector)
    return (routed + side).astype(jnp.bfloat16)


def solution(mesh):
    placed = (
        P(("ep", "tp"), None),
        P(),
        P(("ep", "tp"), None),
        P(("ep", "tp"), None),
        P("ep", None, "tp"),
        P("ep", None, "tp"),
        P("ep", None, "tp"),
        P("ep", None),
        P("ep", None),
        P(None, "ep"),
        P(),
    )
    return jax.shard_map(
        on_device, mesh=mesh, in_specs=placed, out_specs=P(("ep", "tp"), None), check_vma=False
    )
```

time: 153 us -> 146 us (0.954)
  Pallas kernels: 148 us -> 143 us
  local copies, waits for them, and re-layouts: 4.58 us -> 2.3 us
    pallas_call x1, Pallas kernels: 148 us -> 143 us  [fused_layer(): pl.pallas_call(functools.partial(moe_kernel, ne, nz), out_shape=jax.Shape...]
    unnamed x7 -> x1, local copies, waits for them, and re-layouts: 4.58 us -> 2.3 us
where the time goes in v1:
time: 146 us
  Pallas kernels  143 us (98%)
  local copies, waits for them, and re-layouts  2.3 us (2%)
    pallas_call x1, Pallas kernels, fused_layer(): pl.pallas_call(functools.partial(moe_kernel, ne, nz), out_shape=jax.Shape...  143 us

profile of v1, /device:TPU:0, one launch (start us, length us, event | category | flops | bytes accessed | tf_op | source)
XLA Modules:
  0.0 145.5 jit_solution(17140838104960005203)
XLA Ops:
  0.0 143.2 %shard_map.109 = bf16[256,2048]{1,0:T(8,128)(2,1)} custom-call(bf16[256,2048]{1,0:T(8,128)(2,1)} %x_hbm.1, bf16[2048,128]{1,0:T(8,128)(2,1)} %bitcast.7, bf16[2048,128]{1,0:T(8,128)(2,1)} %bitcast.8, bf16[2048,128]{1,0:T(8,128)(2,1)} %bitcast.9, bf16[512,256]{1,0:T(8,128)(2,1)} %dg_hbm.1, bf16[512,256]{1,0:T(8,128)(2,1)} %du_hbm.1, bf16[256,512]{1,0:T(8,128)(2,1)} %dd_hbm.1, ...), custom_call_target="tpu_custom_call" | custom-call | flops 12884901888 | bytes 4194304 | tf_op jit(solution)/shard_map/pallas_call | solution.py:441
  143.2 2.3 %copy.13 = bf16[256,2048]{1,0:T(8,128)(2,1)} copy(bf16[256,2048]{1,0:T(8,128)(2,1)} %shard_map.109) | data formatting | bytes 2097152

commit v2 on v1

--- a/solution.py
+++ b/solution.py
@@ -8,7 +8,7 @@
 from jax.sharding import PartitionSpec as P
 
 MESH = pl.DeviceIdType.MESH
-VMEM_BYTES = 65000 * 1024
+VMEM_BYTES = 64000 * 1024
 CORES = 2
 CHUNK = 256
 SUB = 8
@@ -33,7 +33,6 @@
     across, along, diagonal = me + 1 - 2 * (me % 2), (me + 2) % ne, ne - 1 - me
     peers = [across, along, diagonal]
     partner = z * CORES + (1 - c)
-    inner = (z > 0) & (z < nz - 1)
 
     local = [pltpu.make_async_copy(wg_hbm, ws.at[z, c, 0], lsem.at[0])]
     local.append(pltpu.make_async_copy(wu_hbm, ws.at[z, c, 1], lsem.at[1]))
@@ -58,7 +57,8 @@
         pl.semaphore_signal(barrier, inc=1, device_id={"tp": tp + CORES}, device_id_type=MESH)
 
     neighbours = (z + nz - 1) // nz + (2 * nz - 2 - z) // nz
-    pl.semaphore_wait(barrier, ne + neighbours)
+    with jax.named_scope("barrier"):
+        pl.semaphore_wait(barrier, ne + neighbours)
 
     def remote(src, dst, send, recv, **device):
         return pltpu.make_async_remote_copy(
@@ -168,7 +168,8 @@
         mix_ref[at, :] = 1.0 / (1.0 + jnp.exp(-m))
         return carry
 
-    lax.fori_loop(0, rows // tile, norm, 0)
+    with jax.named_scope("norm"):
+        lax.fori_loop(0, rows // tile, norm, 0)
     local[3].wait()
 
     def own_chunks(j, carry):
@@ -189,11 +190,6 @@
         token_copy(k).start()
     for k in range(ne - 1):
         gate_copy(k, me).start()
-    for p in range(3):
-        local[4 + p].wait()
-    for p in range(3):
-        for k in range(ne - 1):
-            dense_copy(k, p, me).start()
 
     def forward(d, p):
         @pl.when(z >= d)
@@ -241,44 +237,90 @@
         def _():
             fn(z + d)
 
-    def own_chunk(j):
-        @pl.when(inner)
-        def _():
-            c_right(z, j)
-            c_left(z, j)
+    def arrive(src, j):
+        await_chunk(src, c, j)
+        c_partner(src, j)
+
+    def ahead(t):
+        for d in range(nz - 1):
+            j = t + nz - 1 - d
+
+            @pl.when((z == 1) & (j >= 0) & (j < nj))
+            def _():
+                if d == 0:
+                    c_right(z, j)
+                elif d == 1:
+                    arrive(z - 1, j)
+                    c_right(z - 1, j)
+                    arrive(z + 1, j)
+                else:
+                    arrive(z + 2, j)
+                    for src in range(nz - 1):
+                        c_left(z + src, j)
+
+            @pl.when((z == 2) & (j >= 0) & (j < nj))
+            def _():
+                if d == 0:
+                    c_left(z, j)
+                elif d == 1:
+                    arrive(z + 1, j)
+                    c_left(z + 1, j)
+                    arrive(z - 1, j)
+                else:
+                    arrive(z - 2, j)
+                    for src in range(nz - 1):
+                        c_right(z - src, j)
 
     for p in range(2):
-        forward(1, p)
-    for k in range(2):
-        await_token(k)
-        token_copy(2 + k).start()
+        with jax.named_scope(f"forward1_{p}"):
+            forward(1, p)
+    with jax.named_scope("token_relay"):
+        for k in range(2):
+            await_token(k)
+            token_copy(2 + k).start()
+    for p in range(3):
+        local[4 + p].wait()
+        for k in range(ne - 1):
+            dense_copy(k, p, me).start()
     for d in range(2, nz - 1):
         for p in range(2):
-            forward(d, p)
-    for j in range(2):
-        own_chunk(j)
-    for k in range(ne - 1):
-        gate_copy(k, peers[k]).wait_recv()
+            with jax.named_scope(f"forward{d}_{p}"):
+                forward(d, p)
+    ahead(1 - nz)
+    with jax.named_scope("gate_wait"):
+        for k in range(ne - 1):
+            gate_copy(k, peers[k]).wait_recv()
     lane = lax.broadcasted_iota(jnp.int32, (rows, SUB), 1)
     for b in range(ne):
         column = jnp.where(lane == me, wts[b].T, 0.0)
         wcol[b] = jnp.sum(column, axis=1, keepdims=True)
-    for k in range(2, 4):
-        await_token(k)
-    hidden(z)
+    with jax.named_scope("token_wait"):
+        for k in range(2, 4):
+            await_token(k)
+    with jax.named_scope("hidden_own"):
+        hidden(z)
     for d in range(1, nz - 1):
-        both(d, hidden)
-    for k in range(ne - 1):
-        for p in range(3):
-            dense_copy(k, p, peers[k]).wait_recv()
-            dense_partner(k, p, c).start()
-    forward(nz - 1, 0)
-    for k in range(ne - 1):
-        for p in range(3):
-            dense_partner(k, p, 1 - c).wait_recv()
-    dense_side(ne, me, xg, dgs, dus, dds, mix_ref, side)
-    forward(nz - 1, 1)
-    both(nz - 1, hidden)
+        with jax.named_scope(f"ahead{d}"):
+            ahead(d + 1 - nz)
+        with jax.named_scope(f"hidden{d}"):
+            both(d, hidden)
+    with jax.named_scope("dense_wait"):
+        for k in range(ne - 1):
+            for p in range(3):
+                dense_copy(k, p, peers[k]).wait_recv()
+                dense_partner(k, p, c).start()
+    with jax.named_scope("forward_last0"):
+        forward(nz - 1, 0)
+    with jax.named_scope("dense_partner"):
+        for k in range(ne - 1):
+            for p in range(3):
+                dense_partner(k, p, 1 - c).wait_recv()
+    with jax.named_scope("dense_side"):
+        dense_side(ne, me, xg, dgs, dus, dds, mix_ref, side)
+    with jax.named_scope("forward_last1"):
+        forward(nz - 1, 1)
+    with jax.named_scope("hidden_last"):
+        both(nz - 1, hidden)
 
     def back(k, j):
         block = (diagonal, diagonal, across, along, along, across)[k]
@@ -295,30 +337,17 @@
         remote(piece, piece, rsend.at[k], rrecv.at[0, k], ep=across).wait_send()
 
     def take(j):
-        @pl.when(j + 2 < nj)
-        def _():
-            own_chunk(j + 2)
-
-        for d in range(1, nz):
-            @pl.when(z >= d)
-            def _():
-                await_chunk(z - d, c, j)
-
-                @pl.when(z < nz - 1)
-                def _():
-                    c_right(z - d, j)
-
-                c_partner(z - d, j)
-
-            @pl.when(z + d < nz)
-            def _():
-                await_chunk(z + d, c, j)
-
-                @pl.when(z > 0)
-                def _():
-                    c_left(z + d, j)
-
-                c_partner(z + d, j)
+        ahead(j)
+
+        @pl.when(z == 0)
+        def _():
+            for d in range(1, nz):
+                arrive(d, j)
+
+        @pl.when(z == nz - 1)
+        def _():
+            for d in range(1, nz):
+                arrive(z - d, j)
 
         for src in range(nz):
             await_chunk(src, 1 - c, j)
@@ -365,24 +394,32 @@
         out_ref[:, at] = total.astype(jnp.bfloat16)
 
     def step(j, carry):
-        take(j)
-        produce(j)
+        with jax.named_scope("take"):
+            take(j)
+        with jax.named_scope("produce"):
+            produce(j)
 
         @pl.when(j >= 1)
         def _():
-            pass_on(j - 1)
-
-        @pl.when(j >= 2)
-        def _():
-            combine(j - 2)
+            with jax.named_scope("pass_on"):
+                pass_on(j - 1)
+
+        @pl.when((j >= 2) & (j < nj - 1))
+        def _():
+            with jax.named_scope("combine"):
+                combine(j - 2)
 
         return carry
 
     lax.fori_loop(0, nj, step, 0)
-    pass_on(nj - 1)
-    combine(nj - 2)
-    combine(nj - 1)
-
+    with jax.named_scope("pass_on"):
+        pass_on(nj - 1)
+    for j in range(nj - 3, nj):
+        with jax.named_scope("combine"):
+            combine(j)
+
+    drain = jax.named_scope("drain")
+    drain.__enter__()
     for k in range(4):
         token_copy(k).wait_send()
     for k in range(ne - 1):
@@ -408,6 +445,7 @@
         await_sent(src, cpartner)
     for k in range(6):
         await_back(k)
+    drain.__exit__(None, None, None)
 
 
 def dense_side(ne, me, xg, dgs, dus, dds, mix_ref, side):
@@ -440,7 +478,7 @@
     flops = 6 * ne * rows * width * shard * tp
     return pl.pallas_call(
         functools.partial(moe_kernel, ne, nz),
-        out_shape=jax.ShapeDtypeStruct((rows, width), bf),
+        out_shape=pltpu.VMEM((rows, width), bf),
         in_specs=[hbm] * 7 + [vmem] * 4,
         out_specs=vmem,
         scratch_shapes=[
@@ -500,7 +538,7 @@
     size = 2 * ne * block * 2 + 24 * block + 6 * width * shard * tp
     size += 2 * ne * rows * shard * tp + 6 * ne * dense_gate.size + 1024 * ne * rows
     aligned = shard % 128 == 0 and width % (2 * CHUNK) == 0 and rows % 64 == 0
-    return ne == 4 and tp % CORES == 0 and tp > 2 * CORES and aligned and size < VMEM_BYTES * 15 // 16
+    return ne == 4 and tp == 4 * CORES and aligned and size < VMEM_BYTES * 15 // 16
 
 
 def dense_branch(normed, dense_gate, dense_up, dense_down, mix_vector):

time: 146 us -> 121 us (0.83)
  Pallas kernels: 143 us -> 120 us
    pallas_call x1, Pallas kernels: 143 us -> 120 us  [fused_layer(): pl.pallas_call(functools.partial(moe_kernel, ne, nz), out_shape=pltpu.VME...]
where the time goes in v2:
time: 121 us
  Pallas kernels  120 us (99%)
    pallas_call x1, Pallas kernels, fused_layer(): pl.pallas_call(functools.partial(moe_kernel, ne, nz), out_shape=pltpu.VME...  120 us

profile of v2, /device:TPU:0, one launch (start us, length us, event | category | flops | bytes accessed | tf_op | source)
XLA Modules:
  0.0 121.0 jit_solution(2004560637162240049)
XLA Ops:
  0.0 120.0 %shard_map.109 = bf16[256,2048]{1,0:T(8,128)(2,1)S(1)} custom-call(bf16[256,2048]{1,0:T(8,128)(2,1)} %x_hbm.1, bf16[2048,128]{1,0:T(8,128)(2,1)} %bitcast.7, bf16[2048,128]{1,0:T(8,128)(2,1)} %bitcast.8, bf16[2048,128]{1,0:T(8,128)(2,1)} %bitcast.9, bf16[512,256]{1,0:T(8,128)(2,1)} %dg_hbm.1, bf16[512,256]{1,0:T(8,128)(2,1)} %du_hbm.1, ...), custom_call_target="tpu_custom_call" | custom-call | flops 12884901888 | bytes 4194304 | tf_op jit(solution)/shard_map/pallas_call | solution.py:479
  120.0 1.0 copy.13

commit v3 on v2

v3 whole, which is shorter than its diff:
```python
import functools

import jax
import jax.numpy as jnp
from jax import lax
from jax.experimental import pallas as pl
from jax.experimental.pallas import tpu as pltpu
from jax.sharding import PartitionSpec as P

MESH = pl.DeviceIdType.MESH
VMEM_BYTES = 64000 * 1024
CORES = 2
UNIT = 128
SUB = 8
eps = 1e-06


def moe_kernel(
    ne, nz, x_hbm, wg_hbm, wu_hbm, wd_hbm, dg_hbm, du_hbm, dd_hbm, ids_hbm, gates_hbm,
    gain_hbm, mixv_hbm, out_ref,
    xin, xg, ws, dgs, dus, dds, gbuf, hbuf, own, keep, ysend, yrecv, relay, side, mix_ref, wts, wcol,
    ids_ref, gates_ref, gain_ref, mixv_ref,
    lsem, wrecv, wright, wleft, wpartner, crecv, precv,
    tsend, trecv, gsem, dsem, drecv, rsend, rrecv,
):
    me = lax.axis_index("ep")
    tp = lax.axis_index("tp")
    z = tp // CORES
    c = tp % CORES
    rows, width = xg.shape[1], xg.shape[2]
    units = ysend.shape[2]
    nj = crecv.shape[0]
    half = rows // 2
    shard = ws.shape[4]
    across, along, diagonal = me + 1 - 2 * (me % 2), (me + 2) % ne, ne - 1 - me
    peers = [across, along, diagonal]
    partner = z * CORES + (1 - c)

    local = [pltpu.make_async_copy(wg_hbm, ws.at[z, c, 0], lsem.at[0])]
    local.append(pltpu.make_async_copy(wu_hbm, ws.at[z, c, 1], lsem.at[1]))
    local.append(pltpu.make_async_copy(x_hbm, xin, lsem.at[2]))
    local.append(pltpu.make_async_copy(wd_hbm, ws.at[z, c, 2], lsem.at[3]))
    for p, (ref, slot) in enumerate(((dg_hbm, dgs), (du_hbm, dus), (dd_hbm, dds))):
        local.append(pltpu.make_async_copy(ref, slot.at[0], lsem.at[4 + p]))
    smalls = ((ids_hbm, ids_ref), (gates_hbm, gates_ref), (gain_hbm, gain_ref), (mixv_hbm, mixv_ref))
    for p, (ref, slot) in enumerate(smalls):
        local.append(pltpu.make_async_copy(ref, slot, lsem.at[7 + p]))
    for copy in local:
        copy.start()

    barrier = pltpu.get_barrier_semaphore()
    for peer in peers:
        pl.semaphore_signal(barrier, inc=1, device_id={"ep": peer}, device_id_type=MESH)
    pl.semaphore_signal(barrier, inc=1, device_id={"tp": partner}, device_id_type=MESH)

    @pl.when(z > 0)
    def _():
        pl.semaphore_signal(barrier, inc=1, device_id={"tp": tp - CORES}, device_id_type=MESH)

    @pl.when(z < nz - 1)
    def _():
        pl.semaphore_signal(barrier, inc=1, device_id={"tp": tp + CORES}, device_id_type=MESH)

    neighbours = (z + nz - 1) // nz + (2 * nz - 2 - z) // nz
    with jax.named_scope("barrier"):
        pl.semaphore_wait(barrier, ne + neighbours)

    def remote(src, dst, send, recv, **device):
        return pltpu.make_async_remote_copy(
            src_ref=src, dst_ref=dst, send_sem=send, recv_sem=recv,
            device_id=device, device_id_type=MESH,
        )

    def weight_copy(src, p, target, sems):
        piece = ws.at[src, c, p]
        return remote(piece, piece, sems.at[src], wrecv.at[src, c, p], tp=target)

    def to_right(src, p):
        weight_copy(src, p, tp + CORES, wright).start()

    def to_left(src, p):
        weight_copy(src, p, tp - CORES, wleft).start()

    def to_partner(src, p):
        weight_copy(src, p, partner, wpartner).start()

    def await_piece(src, color, p):
        piece = ws.at[src, color, p]
        remote(piece, piece, wpartner.at[src], wrecv.at[src, color, p], tp=partner).wait_recv()

    def await_sent(src, sems):
        piece = ws.at[src, c]
        remote(piece, piece, sems.at[src], wrecv.at[src, c, 0], tp=partner).wait_send()

    def at(j, fn):
        if isinstance(j, int):
            if 0 <= j < nj:
                fn(j, max(2 * j - 1, 0), 1 if j in (0, nj - 1) else 2)
            return
        pl.when(j == 0)(lambda: fn(0, 0, 1))
        pl.when((j > 0) & (j < nj - 1))(lambda: fn(j, 2 * j - 1, 2))
        pl.when(j == nj - 1)(lambda: fn(nj - 1, units - 1, 1))

    def columns(u, n):
        return pl.ds(pl.multiple_of(u * UNIT, UNIT), n * UNIT)

    def chunk_copy(src, target, sems, recv, u, n):
        piece = ws.at[src, c, 2, columns(u, n)]
        remote(piece, piece, sems.at[src], recv, tp=target).start()

    def c_right(src, j, u, n):
        chunk_copy(src, tp + CORES, wright, crecv.at[j, src], u, n)

    def c_left(src, j, u, n):
        chunk_copy(src, tp - CORES, wleft, crecv.at[j, src], u, n)

    def c_partner(src, j, u, n):
        chunk_copy(src, partner, wpartner, precv.at[j], u, n)

    def arrive(src, j, u, n):
        piece = ws.at[src, c, 2, columns(u, n)]
        remote(piece, piece, wpartner.at[src], crecv.at[j, src], tp=partner).wait_recv()
        c_partner(src, j, u, n)

    def token_copy(k):
        block = (me, me, across, along)[k]
        peer = (across, along, along, across)[k]
        low, size = ((0, rows), (0, rows), (0, half), (half, half))[k]
        piece = xg.at[block, low : low + size]
        return remote(piece, piece, tsend.at[k], trecv.at[k], ep=peer)

    def await_token(k):
        block = (across, along, diagonal, diagonal)[k]
        low, size = ((0, rows), (0, rows), (0, half), (half, half))[k]
        piece = xg.at[block, low : low + size]
        remote(piece, piece, tsend.at[k], trecv.at[k], ep=across).wait_recv()

    def gate_copy(k):
        return remote(wts.at[0], wts.at[1 + k], gsem.at[0], gsem.at[1 + k], ep=peers[k])

    def gate_all():
        piece = wts.at[1:]
        return remote(piece, piece, gsem.at[0], gsem.at[1], ep=across)

    def await_gate(k):
        piece = wts.at[1 + k]
        remote(piece, piece, gsem.at[0], gsem.at[1 + k], ep=across).wait_recv()

    def dense_piece(p, blocks, color):
        slot = (dgs, dus, dds)[p]
        part = slot.shape[1] // CORES
        return slot.at[blocks, pl.ds(pl.multiple_of(color * part, part), part)]

    def dense_copy(k, p):
        lands = dense_piece(p, 1 + k, c)
        return remote(dense_piece(p, 0, c), lands, dsem.at[p], drecv.at[k, p], ep=peers[k])

    def dense_partner(k, p, color):
        piece = dense_piece(p, 1 + k, color)
        return remote(piece, piece, dsem.at[3 + p], drecv.at[ne - 1 + k, p], tp=partner)

    def dense_sent(p):
        piece = dense_piece(p, pl.ds(1, ne - 1), c)
        for first in (0, 3):
            remote(piece, piece, dsem.at[first + p], drecv.at[0, p], tp=partner).wait_send()

    for p in range(2):
        local[p].wait()

        @pl.when(z < nz - 1)
        def _():
            to_right(z, p)

        @pl.when(z > 0)
        def _():
            to_left(z, p)

        to_partner(z, p)
    for p in (2, 7, 8, 9, 10):
        local[p].wait()

    expert = lax.broadcasted_iota(jnp.int32, (SUB, rows), 0)
    named, gate = ids_ref[...], gates_ref[...]
    weight = jnp.zeros((SUB, rows), jnp.float32)
    for k in range(ids_ref.shape[0]):
        weight += jnp.where(named[k : k + 1, :] == expert, gate[k : k + 1, :], 0.0)
    wts[0] = weight
    tile = 32

    def norm(i, carry):
        at = pl.ds(pl.multiple_of(i * tile, tile), tile)
        v = xin[at, :].astype(jnp.float32)
        scale = lax.rsqrt(jnp.sum(v * v, axis=1, keepdims=True) * (1.0 / width) + eps)
        n = (v * scale * gain_ref[...]).astype(jnp.bfloat16)
        xg[me, at, :] = n
        m = jnp.sum(n.astype(jnp.float32) * mixv_ref[...], axis=1, keepdims=True)
        mix_ref[at, :] = 1.0 / (1.0 + jnp.exp(-m))
        return carry

    with jax.named_scope("norm"):
        lax.fori_loop(0, rows // tile, norm, 0)
    local[3].wait()

    def own_chunk(j, u, n):
        c_partner(z, j, u, n)

        @pl.when(z == 0)
        def _():
            c_right(z, j, u, n)

        @pl.when(z == nz - 1)
        def _():
            c_left(z, j, u, n)

    def own_chunks(j, carry):
        at(j, own_chunk)
        return carry

    lax.fori_loop(0, nj, own_chunks, 0)
    for k in range(2):
        token_copy(k).start()
    for k in range(ne - 1):
        gate_copy(k).start()

    def forward(d, p):
        @pl.when(z >= d)
        def _():
            await_piece(z - d, c, p)

            @pl.when(z < nz - 1)
            def _():
                to_right(z - d, p)

            to_partner(z - d, p)

        @pl.when(z + d < nz)
        def _():
            await_piece(z + d, c, p)

            @pl.when(z > 0)
            def _():
                to_left(z + d, p)

            to_partner(z + d, p)

    def weight_of(src, p):
        return jnp.concatenate([ws[src, i, p] for i in range(CORES)], axis=1)

    def gate_part(src):
        await_piece(src, 1 - c, 0)

        def one(b, carry):
            g = jnp.dot(xg[b], weight_of(src, 0), preferred_element_type=jnp.float32)
            gbuf[b] = g / (1.0 + jnp.exp(-g)) * wcol[b]
            return carry

        lax.fori_loop(0, ne, one, 0)

    def up_part(src):
        await_piece(src, 1 - c, 1)
        here = pl.ds(pl.multiple_of(src * (CORES * shard), CORES * shard), CORES * shard)

        def one(b, carry):
            u = jnp.dot(xg[b], weight_of(src, 1), preferred_element_type=jnp.float32)
            hbuf[b, :, here] = (gbuf[b] * u).astype(jnp.bfloat16)
            return carry

        lax.fori_loop(0, ne, one, 0)

    def hidden(src):
        gate_part(src)
        up_part(src)

    def both(d, fn):
        @pl.when(z >= d)
        def _():
            fn(z - d)

        @pl.when(z + d < nz)
        def _():
            fn(z + d)

    def ahead(t):
        def one(d, j, u, n):
            @pl.when(z == 1)
            def _():
                if d == 0:
                    c_right(z, j, u, n)
                elif d == 1:
                    arrive(z - 1, j, u, n)
                    c_right(z - 1, j, u, n)
                    arrive(z + 1, j, u, n)
                else:
                    arrive(z + 2, j, u, n)
                    for src in range(nz - 1):
                        c_left(z + src, j, u, n)

            @pl.when(z == 2)
            def _():
                if d == 0:
                    c_left(z, j, u, n)
                elif d == 1:
                    arrive(z + 1, j, u, n)
                    c_left(z + 1, j, u, n)
                    arrive(z - 1, j, u, n)
                else:
                    arrive(z - 2, j, u, n)
                    for src in range(nz - 1):
                        c_right(z - src, j, u, n)

        for d in range(nz - 1):
            at(t + nz - 1 - d, functools.partial(one, d))

    for p in range(2):
        with jax.named_scope(f"forward1_{p}"):
            forward(1, p)
    with jax.named_scope("token_relay"):
        for k in range(2):
            await_token(k)
            token_copy(2 + k).start()
    for p in range(3):
        local[4 + p].wait()
        for k in range(ne - 1):
            dense_copy(k, p).start()
    for d in range(2, nz - 1):
        for p in range(2):
            with jax.named_scope(f"forward{d}_{p}"):
                forward(d, p)
    ahead(1 - nz)
    with jax.named_scope("gate_wait"):
        for k in range(ne - 1):
            await_gate(k)
    lane = lax.broadcasted_iota(jnp.int32, (rows, SUB), 1)
    for r, b in enumerate([me] + peers):
        column = jnp.where(lane == me, wts[r].T, 0.0)
        wcol[b] = jnp.sum(column, axis=1, keepdims=True)
    with jax.named_scope("token_wait"):
        for k in range(2, 4):
            await_token(k)
    with jax.named_scope("hidden_own"):
        hidden(z)
    for d in range(1, nz - 1):
        with jax.named_scope(f"ahead{d}"):
            ahead(d + 1 - nz)
        with jax.named_scope(f"hidden{d}"):
            both(d, hidden)
    with jax.named_scope("dense_wait"):
        for p in range(3):
            for k in range(ne - 1):
                dense_copy(k, p).wait_recv()
                dense_partner(k, p, c).start()
    with jax.named_scope("forward_last0"):
        forward(nz - 1, 0)
    with jax.named_scope("gate_last"):
        both(nz - 1, gate_part)
    with jax.named_scope("dense_partner"):
        for p in range(3):
            for k in range(ne - 1):
                dense_partner(k, p, 1 - c).wait_recv()
    with jax.named_scope("dense_side"):
        dense_side([me] + peers, me, xg, dgs, dus, dds, mix_ref, side)
    with jax.named_scope("forward_last1"):
        forward(nz - 1, 1)
    with jax.named_scope("up_last"):
        both(nz - 1, up_part)

    def back(k, j, u, n):
        block = (diagonal, diagonal, across, along, along, across)[k]
        peer = (across, along, across, along, along, across)[k]
        spot = (0, 1, 0, 1, 1, 0)[k]
        to = pl.ds(u, n)
        lands = relay.at[k, to] if k < 2 else yrecv.at[spot, k % 2, to]
        piece = ysend.at[block, k % 2, to]
        return remote(piece, lands, rsend.at[0], rrecv.at[j, min(k, 2)], ep=peer)

    def await_back(j, u, n):
        piece = yrecv.at[:, :, pl.ds(u, n)]
        remote(piece, piece, rsend.at[0], rrecv.at[j, 2], ep=across).wait_recv()

    def take(j, u, n):
        ahead(j)

        @pl.when(z == 0)
        def _():
            for d in range(1, nz):
                arrive(d, j, u, n)

        @pl.when(z == nz - 1)
        def _():
            for d in range(1, nz):
                arrive(z - d, j, u, n)

        piece = ws.at[:, 1 - c, 2, columns(u, n)]
        remote(piece, piece, wpartner.at[0], precv.at[j], tp=partner).wait_recv()

    def produce(j, u, n):
        here = columns(u, n)
        w = jnp.concatenate([ws[s, i, 2, here, :] for s in range(nz) for i in range(CORES)], axis=1)

        def rows_of(b):
            return lax.dot_general(
                hbuf[b], w, (((1,), (1,)), ((), ())), preferred_element_type=jnp.float32
            )

        def put(y, *lead):
            ref, lead = lead[0], lead[1:]
            for i in range(n):
                ref[lead + (u + i,)] = y[:, i * UNIT : (i + 1) * UNIT].astype(ref.dtype)

        y = rows_of(diagonal)
        for k in range(2):
            put(y[k * half : (k + 1) * half], ysend, diagonal, k)
            back(k, j, u, n).start()
        y = rows_of(across)
        put(y[:half], ysend, across, 0)
        put(y[half:], keep, 1)
        back(2, j, u, n).start()
        y = rows_of(along)
        put(y[half:], ysend, along, 1)
        put(y[:half], keep, 0)
        back(3, j, u, n).start()
        own[:, here] = rows_of(me)

    def pass_on(j, u, n):
        for k, block in enumerate((along, across)):
            back(k, j, u, n).wait_recv()
            for i in range(n):
                v = keep[k, u + i] + relay[k, u + i].astype(jnp.float32)
                ysend[block, k, u + i] = v.astype(jnp.bfloat16)
            back(4 + k, j, u, n).start()

    def combine(j, u, n):
        await_back(j, u, n)
        for i in range(n):
            here = columns(u + i, 1)
            for h in range(2):
                low = h * half
                total = side[low : low + half, here] + own[low : low + half, here]
                for k in range(2):
                    total = total + yrecv[k, h, u + i].astype(jnp.float32)
                out_ref[low : low + half, here] = total.astype(jnp.bfloat16)

    def scoped(name, j, fn):
        with jax.named_scope(name):
            at(j, fn)

    def step(j, carry):
        take(j, 2 * j - 1, 2)
        with jax.named_scope("produce"):
            produce(j, 2 * j - 1, 2)
        scoped("pass_on", j - 1, pass_on)
        scoped("combine", j - 2, combine)
        return carry

    scoped("take", 0, take)
    scoped("produce", 0, produce)
    lax.fori_loop(1, nj - 1, step, 0)
    scoped("take", nj - 1, take)
    scoped("produce", nj - 1, produce)
    scoped("pass_on", nj - 2, pass_on)
    scoped("pass_on", nj - 1, pass_on)
    for j in range(nj - 3, nj):
        scoped("combine", j, combine)

    drain = jax.named_scope("drain")
    drain.__enter__()
    for k in range(4):
        token_copy(k).wait_send()
    gate_all().wait_send()
    for p in range(3):
        dense_sent(p)
    for src in range(nz):
        @pl.when((z < nz - 1) & (z >= src))
        def _():
            await_sent(src, wright)

        @pl.when((z > 0) & (z <= src))
        def _():
            await_sent(src, wleft)

        await_sent(src, wpartner)
    piece = ysend.at[: ne - 1]
    remote(piece, piece, rsend.at[0], rrecv.at[0, 0], ep=across).wait_send()
    drain.__exit__(None, None, None)


def dense_side(owners, me, xg, dgs, dus, dds, mix_ref, side):
    deep, wide = dgs.shape[1], dds.shape[2]
    g = u = None
    for r, e in enumerate(owners):
        x = xg[me, :, pl.ds(pl.multiple_of(e * deep, deep), deep)]
        ge = jnp.dot(x, dgs[r], preferred_element_type=jnp.float32)
        ue = jnp.dot(x, dus[r], preferred_element_type=jnp.float32)
        g, u = (ge, ue) if r == 0 else (g + ge, u + ue)
    h = (g / (1.0 + jnp.exp(-g)) * u).astype(jnp.bfloat16)
    for r, e in enumerate(owners):
        o = jnp.dot(h, dds[r], preferred_element_type=jnp.float32)
        side[:, pl.ds(pl.multiple_of(e * wide, wide), wide)] = mix_ref[...] * o


def fused_layer(
    ne, tp, tokens, norm_gain, expert_ids, gate_weights,
    w_gate, w_up, w_down, dense_gate, dense_up, dense_down, mix_vector,
):
    nz = tp // CORES
    rows, width = tokens.shape
    topk = expert_ids.shape[1]
    shard = w_gate.shape[2]
    units = width // UNIT
    nj = units // 2 + 1
    half = rows // 2
    bf, f32 = jnp.bfloat16, jnp.float32
    dma = pltpu.SemaphoreType.DMA
    hbm = pl.BlockSpec(memory_space=pl.ANY)
    vmem = pl.BlockSpec(memory_space=pltpu.VMEM)
    flops = 6 * ne * rows * width * shard * tp
    return pl.pallas_call(
        functools.partial(moe_kernel, ne, nz),
        out_shape=pltpu.VMEM((rows, width), bf),
        in_specs=[hbm] * 11,
        out_specs=vmem,
        scratch_shapes=[
            pltpu.VMEM((rows, width), bf),
            pltpu.VMEM((ne, rows, width), bf),
            pltpu.VMEM((nz, CORES, 3, width, shard), bf),
            pltpu.VMEM((ne,) + dense_gate.shape, bf),
            pltpu.VMEM((ne,) + dense_up.shape, bf),
            pltpu.VMEM((ne,) + dense_down.shape, bf),
            pltpu.VMEM((ne, rows, CORES * shard), f32),
            pltpu.VMEM((ne, rows, tp * shard), bf),
            pltpu.VMEM((rows, width), f32),
            pltpu.VMEM((2, units, half, UNIT), f32),
            pltpu.VMEM((ne, 2, units, half, UNIT), bf),
            pltpu.VMEM((2, 2, units, half, UNIT), bf),
            pltpu.VMEM((2, units, half, UNIT), bf),
            pltpu.VMEM((rows, width), f32),
            pltpu.VMEM((rows, 1), f32),
            pltpu.VMEM((ne, SUB, rows), f32),
            pltpu.VMEM((ne, rows, 1), f32),
            pltpu.VMEM((topk, rows), jnp.int32),
            pltpu.VMEM((topk, rows), f32),
            pltpu.VMEM((1, width), f32),
            pltpu.VMEM((1, width), f32),
            dma((11,)),
            dma((nz, CORES, 2)),
            dma((nz,)),
            dma((nz,)),
            dma((nz,)),
            dma((nj, nz)),
            dma((nj,)),
            dma((4,)),
            dma((4,)),
            dma((ne,)),
            dma((6,)),
            dma((2 * ne - 2, 3)),
            dma((1,)),
            dma((nj, 3)),
        ],
        compiler_params=pltpu.CompilerParams(
            collective_id=0, has_side_effects=True, vmem_limit_bytes=VMEM_BYTES
        ),
        cost_estimate=pl.CostEstimate(
            flops=flops, bytes_accessed=8 * rows * width, transcendentals=ne * rows * shard * tp
        ),
    )(
        tokens, w_gate[0], w_up[0], w_down[0], dense_gate, dense_up, dense_down,
        expert_ids.T, gate_weights.T, norm_gain.reshape(1, width), mix_vector.reshape(1, width),
    )


def fits(ne, tp, tokens, w_gate, dense_gate):
    rows, width = tokens.shape
    shard = w_gate.shape[2]
    block = rows * width
    size = 2 * ne * block * 2 + 24 * block + 6 * width * shard * tp
    size += 2 * ne * rows * shard * tp + 6 * ne * dense_gate.size + 1024 * ne * rows
    size += 8 * ne * rows * shard
    aligned = shard % 128 == 0 and width % (2 * UNIT) == 0 and rows % 64 == 0
    return ne == 4 and tp == 4 * CORES and aligned and size < VMEM_BYTES * 15 // 16


def dense_branch(normed, dense_gate, dense_up, dense_down, mix_vector):
    dense_g = jnp.dot(
        normed,
        lax.all_gather(dense_gate, "ep", axis=0, tiled=True),
        preferred_element_type=jnp.float32,
    )
    dense_u = jnp.dot(
        normed,
        lax.all_gather(dense_up, "ep", axis=0, tiled=True),
        preferred_element_type=jnp.float32,
    )
    dense_hidden = (jax.nn.silu(dense_g) * dense_u).astype(jnp.bfloat16)
    dense_out = jnp.dot(
        dense_hidden,
        lax.all_gather(dense_down, "ep", axis=1, tiled=True),
        preferred_element_type=jnp.float32,
    )
    mix = jax.nn.sigmoid(jnp.sum(normed.astype(jnp.float32) * mix_vector, axis=1))
    return mix[:, None] * dense_out


def on_device(
    tokens,
    norm_gain,
    expert_ids,
    gate_weights,
    w_gate,
    w_up,
    w_down,
    dense_gate,
    dense_up,
    dense_down,
    mix_vector,
):
    groups = lax.axis_size("ep")
    ring = lax.axis_size("tp")
    if fits(groups, ring, tokens, w_gate, dense_gate):
        return fused_layer(
            groups, ring, tokens, norm_gain, expert_ids, gate_weights,
            w_gate, w_up, w_down, dense_gate, dense_up, dense_down, mix_vector,
        )
    values = tokens.astype(jnp.float32)
    scale = lax.rsqrt(jnp.mean(values * values, axis=1, keepdims=True) + eps)
    normed = (values * scale * norm_gain).astype(jnp.bfloat16)
    count_tok, topk = expert_ids.shape
    width = tokens.shape[1]
    capacity = 2 * count_tok * topk // groups
    flat_ids = expert_ids.reshape(-1)
    onehot = (flat_ids[:, None] == jnp.arange(groups, dtype=jnp.int32)[None, :]).astype(jnp.int32)
    before = jnp.cumsum(onehot, axis=0) - onehot
    slot = jnp.sum(before * onehot, axis=1)
    dest = flat_ids * capacity + slot
    owner = jnp.arange(count_tok * topk, dtype=jnp.int32) // topk
    buffer = jnp.zeros((groups * capacity, width), jnp.bfloat16).at[dest].set(normed[owner])
    arrived = lax.all_to_all(
        buffer.reshape(groups, capacity, width), "ep", split_axis=0, concat_axis=0, tiled=True
    )
    rows = arrived.reshape(groups * capacity, width)
    gate = jnp.dot(
        rows,
        lax.all_gather(w_gate, "tp", axis=2, tiled=True)[0],
        preferred_element_type=jnp.float32,
    )
    upper = jnp.dot(
        rows, lax.all_gather(w_up, "tp", axis=2, tiled=True)[0], preferred_element_type=jnp.float32
    )
    hidden_all = (jax.nn.silu(gate) * upper).astype(jnp.bfloat16)
    expert_out = lax.dot_general(
        hidden_all,
        lax.all_gather(w_down, "tp", axis=2, tiled=True)[0],
        (((1,), (1,)), ((), ())),
        preferred_element_type=jnp.float32,
    )
    results = expert_out.astype(jnp.bfloat16).reshape(groups, capacity, width)
    returned = lax.all_to_all(results, "ep", split_axis=0, concat_axis=0, tiled=True)
    picked = returned.reshape(groups * capacity, width)[dest].reshape(count_tok, topk, width)
    routed = jnp.einsum("tk,tkd->td", gate_weights, picked.astype(jnp.float32))
    side = dense_branch(normed, dense_gate, dense_up, dense_down, mix_vector)
    return (routed + side).astype(jnp.bfloat16)


def solution(mesh):
    placed = (
        P(("ep", "tp"), None),
        P(),
        P(("ep", "tp"), None),
        P(("ep", "tp"), None),
        P("ep", None, "tp"),
        P("ep", None, "tp"),
        P("ep", None, "tp"),
        P("ep", None),
        P("ep", None),
        P(None, "ep"),
        P(),
    )
    return jax.shard_map(
        on_device, mesh=mesh, in_specs=placed, out_specs=P(("ep", "tp"), None), check_vma=False
    )
```

time: 121 us -> 120 us (level)
    pallas_call x1, Pallas kernels: 120 us -> 119 us  [fused_layer(): pl.pallas_call(functools.partial(moe_kernel, ne, nz), out_shape=pltpu.VME...]
where the time goes in v3:
time: 120 us
  Pallas kernels  119 us (99%)
    pallas_call x1, Pallas kernels, fused_layer(): pl.pallas_call(functools.partial(moe_kernel, ne, nz), out_shape=pltpu.VME...  119 us

profile of v3, /device:TPU:0, one launch (start us, length us, event | category | flops | bytes accessed | tf_op | source)
XLA Modules:
  0.0 119.5 jit_solution(14380153076753288420)
XLA Ops:
  0.0 118.5 %shard_map.109 = bf16[256,2048]{1,0:T(8,128)(2,1)S(1)} custom-call(bf16[256,2048]{1,0:T(8,128)(2,1)} %x_hbm.1, bf16[2048,128]{1,0:T(8,128)(2,1)} %bitcast.7, bf16[2048,128]{1,0:T(8,128)(2,1)} %bitcast.8, bf16[2048,128]{1,0:T(8,128)(2,1)} %bitcast.9, bf16[512,256]{1,0:T(8,128)(2,1)} %dg_hbm.1, bf16[512,256]{1,0:T(8,128)(2,1)} %du_hbm.1, ...), custom_call_target="tpu_custom_call" | custom-call | flops 12884901888 | bytes 4194304 | tf_op jit(solution)/shard_map/pallas_call | solution.py:517
  118.5 1.0 copy.13

commit v4 on v3

--- a/solution.py
+++ b/solution.py
@@ -11,6 +11,7 @@
 VMEM_BYTES = 64000 * 1024
 CORES = 2
 UNIT = 128
+TAIL = 256
 SUB = 8
 eps = 1e-06
 
@@ -20,7 +21,7 @@
     gain_hbm, mixv_hbm, out_ref,
     xin, xg, ws, dgs, dus, dds, gbuf, hbuf, own, keep, ysend, yrecv, relay, side, mix_ref, wts, wcol,
     ids_ref, gates_ref, gain_ref, mixv_ref,
-    lsem, wrecv, wright, wleft, wpartner, crecv, precv,
+    lsem, wrecv, wright, wleft, wpartner, xsend, xrecv, crecv, precv,
     tsend, trecv, gsem, dsem, drecv, rsend, rrecv,
 ):
     me = lax.axis_index("ep")
@@ -49,7 +50,7 @@
         copy.start()
 
     barrier = pltpu.get_barrier_semaphore()
-    for peer in peers:
+    for peer in (across, along):
         pl.semaphore_signal(barrier, inc=1, device_id={"ep": peer}, device_id_type=MESH)
     pl.semaphore_signal(barrier, inc=1, device_id={"tp": partner}, device_id_type=MESH)
 
@@ -63,7 +64,7 @@
 
     neighbours = (z + nz - 1) // nz + (2 * nz - 2 - z) // nz
     with jax.named_scope("barrier"):
-        pl.semaphore_wait(barrier, ne + neighbours)
+        pl.semaphore_wait(barrier, 3 + neighbours)
 
     def remote(src, dst, send, recv, **device):
         return pltpu.make_async_remote_copy(
@@ -88,9 +89,21 @@
         piece = ws.at[src, color, p]
         remote(piece, piece, wpartner.at[src], wrecv.at[src, color, p], tp=partner).wait_recv()
 
-    def await_sent(src, sems):
-        piece = ws.at[src, c]
+    def await_sent(src, sems, count):
+        piece = ws.at[src, c, :count]
         remote(piece, piece, sems.at[src], wrecv.at[src, c, 0], tp=partner).wait_send()
+
+    def far_main(src, color, target):
+        piece = ws.at[src, color, 1] if color else ws.at[src, 0, 1, : width - TAIL]
+        return remote(piece, piece, xsend.at[0], wrecv.at[src, color, 1], tp=target)
+
+    def far_tail(src, target):
+        piece = ws.at[src, 0, 1, width - TAIL :]
+        return remote(piece, piece, xsend.at[1], xrecv.at[0], tp=target)
+
+    def by_color(fn):
+        for color in range(CORES):
+            pl.when(c == color)(functools.partial(fn, color))
 
     def at(j, fn):
         if isinstance(j, int):
@@ -219,7 +232,7 @@
     lax.fori_loop(0, nj, own_chunks, 0)
     for k in range(2):
         token_copy(k).start()
-    for k in range(ne - 1):
+    for k in range(2):
         gate_copy(k).start()
 
     def forward(d, p):
@@ -229,7 +242,10 @@
 
             @pl.when(z < nz - 1)
             def _():
-                to_right(z - d, p)
+                if d == nz - 2 and p == 1:
+                    by_color(lambda color: far_main(z - d, color, tp + CORES).start())
+                else:
+                    to_right(z - d, p)
 
             to_partner(z - d, p)
 
@@ -239,7 +255,10 @@
 
             @pl.when(z > 0)
             def _():
-                to_left(z + d, p)
+                if d == nz - 2 and p == 1:
+                    by_color(lambda color: far_main(z + d, color, tp - CORES).start())
+                else:
+                    to_left(z + d, p)
 
             to_partner(z + d, p)
 
@@ -256,8 +275,40 @@
 
         lax.fori_loop(0, ne, one, 0)
 
-    def up_part(src):
-        await_piece(src, 1 - c, 1)
+    def far_forward():
+        src = nz - 1 - z
+
+        def one(color):
+            far_main(src, color, partner).wait_recv()
+            far_main(src, color, partner).start()
+            if color:
+                far_tail(src, partner).wait_recv()
+                far_tail(src, partner).start()
+
+        by_color(one)
+
+    def far_await(src):
+        def one(color):
+            far_main(src, 1 - color, partner).wait_recv()
+            if not color:
+                far_tail(src, partner).wait_recv()
+
+        by_color(one)
+
+    def up_part(src, far=False):
+        if far:
+            far_await(src)
+        else:
+            await_piece(src, 1 - c, 1)
+
+            @pl.when((c == 1) & (z == 1) & (src == nz - 1))
+            def _():
+                far_tail(src, tp - CORES).start()
+
+            @pl.when((c == 1) & (z == nz - 2) & (src == 0))
+            def _():
+                far_tail(src, tp + CORES).start()
+
         here = pl.ds(pl.multiple_of(src * (CORES * shard), CORES * shard), CORES * shard)
 
         def one(b, carry):
@@ -318,6 +369,7 @@
         for k in range(2):
             await_token(k)
             token_copy(2 + k).start()
+    gate_copy(2).start()
     for p in range(3):
         local[4 + p].wait()
         for k in range(ne - 1):
@@ -340,10 +392,10 @@
     with jax.named_scope("hidden_own"):
         hidden(z)
     for d in range(1, nz - 1):
+        with jax.named_scope(f"hidden{d}"):
+            both(d, hidden)
         with jax.named_scope(f"ahead{d}"):
             ahead(d + 1 - nz)
-        with jax.named_scope(f"hidden{d}"):
-            both(d, hidden)
     with jax.named_scope("dense_wait"):
         for p in range(3):
             for k in range(ne - 1):
@@ -360,9 +412,9 @@
     with jax.named_scope("dense_side"):
         dense_side([me] + peers, me, xg, dgs, dus, dds, mix_ref, side)
     with jax.named_scope("forward_last1"):
-        forward(nz - 1, 1)
+        pl.when((z == 0) | (z == nz - 1))(far_forward)
     with jax.named_scope("up_last"):
-        both(nz - 1, up_part)
+        both(nz - 1, functools.partial(up_part, far=True))
 
     def back(k, j, u, n):
         block = (diagonal, diagonal, across, along, along, across)[k]
@@ -470,15 +522,20 @@
     for p in range(3):
         dense_sent(p)
     for src in range(nz):
-        @pl.when((z < nz - 1) & (z >= src))
-        def _():
-            await_sent(src, wright)
-
-        @pl.when((z > 0) & (z <= src))
-        def _():
-            await_sent(src, wleft)
-
-        await_sent(src, wpartner)
+        for sems, there, far in (
+            (wright, (z < nz - 1) & (z >= src), (z == nz - 2) & (src == 0)),
+            (wleft, (z > 0) & (z <= src), (z == 1) & (src == nz - 1)),
+            (wpartner, z >= 0, (z == nz - 1 - src) & (src % (nz - 1) == 0)),
+        ):
+            pl.when(there & far)(functools.partial(await_sent, src, sems, 2))
+            pl.when(there & jnp.logical_not(far))(functools.partial(await_sent, src, sems, 3))
+
+    def far_sent(color):
+        far_main(0, color, partner).wait_send()
+        if color:
+            far_tail(0, partner).wait_send()
+
+    by_color(far_sent)
     piece = ysend.at[: ne - 1]
     remote(piece, piece, rsend.at[0], rrecv.at[0, 0], ep=across).wait_send()
     drain.__exit__(None, None, None)
@@ -546,6 +603,8 @@
             dma((nz,)),
             dma((nz,)),
             dma((nz,)),
+            dma((2,)),
+            dma((1,)),
             dma((nj, nz)),
             dma((nj,)),
             dma((4,)),
@@ -575,7 +634,7 @@
     size = 2 * ne * block * 2 + 24 * block + 6 * width * shard * tp
     size += 2 * ne * rows * shard * tp + 6 * ne * dense_gate.size + 1024 * ne * rows
     size += 8 * ne * rows * shard
-    aligned = shard % 128 == 0 and width % (2 * UNIT) == 0 and rows % 64 == 0
+    aligned = shard % 128 == 0 and width % (2 * UNIT) == 0 and width > TAIL and rows % 64 == 0
     return ne == 4 and tp == 4 * CORES and aligned and size < VMEM_BYTES * 15 // 16
 
 

time: 120 us -> 119 us (level)
  no operation moved by 1% of the time
where the time goes in v4:
time: 119 us
  Pallas kernels  118 us (99%)
    pallas_call x1, Pallas kernels, fused_layer(): pl.pallas_call(functools.partial(moe_kernel, ne, nz), out_shape=pltpu.VME...  118 us

profile of v4, /device:TPU:0, one launch (start us, length us, event | category | flops | bytes accessed | tf_op | source)
XLA Modules:
  0.0 119.1 jit_solution(3444562706939358481)
XLA Ops:
  0.0 118.2 %shard_map.109 = bf16[256,2048]{1,0:T(8,128)(2,1)S(1)} custom-call(bf16[256,2048]{1,0:T(8,128)(2,1)} %x_hbm.1, bf16[2048,128]{1,0:T(8,128)(2,1)} %bitcast.7, bf16[2048,128]{1,0:T(8,128)(2,1)} %bitcast.8, bf16[2048,128]{1,0:T(8,128)(2,1)} %bitcast.9, bf16[512,256]{1,0:T(8,128)(2,1)} %dg_hbm.1, bf16[512,256]{1,0:T(8,128)(2,1)} %du_hbm.1, ...), custom_call_target="tpu_custom_call" | custom-call | flops 12884901888 | bytes 4194304 | tf_op jit(solution)/shard_map/pallas_call | solution.py:574
  118.2 1.0 copy.13

commit v5 on v4

--- a/solution.py
+++ b/solution.py
@@ -11,6 +11,8 @@
 VMEM_BYTES = 64000 * 1024
 CORES = 2
 UNIT = 128
+LOOK = 2
+BEHIND = 2
 TAIL = 256
 SUB = 8
 eps = 1e-06
@@ -29,7 +31,6 @@
     z = tp // CORES
     c = tp % CORES
     rows, width = xg.shape[1], xg.shape[2]
-    units = ysend.shape[2]
     nj = crecv.shape[0]
     half = rows // 2
     shard = ws.shape[4]
@@ -106,34 +107,33 @@
             pl.when(c == color)(functools.partial(fn, color))
 
     def at(j, fn):
-        if isinstance(j, int):
-            if 0 <= j < nj:
-                fn(j, max(2 * j - 1, 0), 1 if j in (0, nj - 1) else 2)
-            return
-        pl.when(j == 0)(lambda: fn(0, 0, 1))
-        pl.when((j > 0) & (j < nj - 1))(lambda: fn(j, 2 * j - 1, 2))
-        pl.when(j == nj - 1)(lambda: fn(nj - 1, units - 1, 1))
-
-    def columns(u, n):
-        return pl.ds(pl.multiple_of(u * UNIT, UNIT), n * UNIT)
-
-    def chunk_copy(src, target, sems, recv, u, n):
-        piece = ws.at[src, c, 2, columns(u, n)]
-        remote(piece, piece, sems.at[src], recv, tp=target).start()
-
-    def c_right(src, j, u, n):
-        chunk_copy(src, tp + CORES, wright, crecv.at[j, src], u, n)
-
-    def c_left(src, j, u, n):
-        chunk_copy(src, tp - CORES, wleft, crecv.at[j, src], u, n)
-
-    def c_partner(src, j, u, n):
-        chunk_copy(src, partner, wpartner, precv.at[j], u, n)
-
-    def arrive(src, j, u, n):
-        piece = ws.at[src, c, 2, columns(u, n)]
-        remote(piece, piece, wpartner.at[src], crecv.at[j, src], tp=partner).wait_recv()
-        c_partner(src, j, u, n)
+        if not isinstance(j, int):
+            pl.when((j >= 0) & (j < nj))(lambda: fn(j))
+        elif 0 <= j < nj:
+            fn(j)
+
+    def columns(j):
+        return pl.ds(pl.multiple_of(j * UNIT, UNIT), UNIT)
+
+    def chunk_copy(src, j, target, sems, recv):
+        piece = ws.at[src, c, 2, columns(j)]
+        return remote(piece, piece, sems.at[src], recv, tp=target)
+
+    def order(src, there):
+        return (src - there + nz) % nz - 1
+
+    def c_right(src, j):
+        chunk_copy(src, j, tp + CORES, wright, crecv.at[j, order(src, z + 1)]).start()
+
+    def c_left(src, j):
+        chunk_copy(src, j, tp - CORES, wleft, crecv.at[j, order(src, z - 1)]).start()
+
+    def c_partner(src, j):
+        chunk_copy(src, j, partner, wpartner, precv.at[j]).start()
+
+    def arrive(src, j):
+        chunk_copy(src, j, partner, wpartner, crecv.at[j, order(src, z)]).wait_recv()
+        c_partner(src, j)
 
     def token_copy(k):
         block = (me, me, across, along)[k]
@@ -214,19 +214,17 @@
         lax.fori_loop(0, rows // tile, norm, 0)
     local[3].wait()
 
-    def own_chunk(j, u, n):
-        c_partner(z, j, u, n)
+    def own_chunks(j, carry):
+        c_partner(z, j)
 
         @pl.when(z == 0)
         def _():
-            c_right(z, j, u, n)
+            c_right(z, j)
 
         @pl.when(z == nz - 1)
         def _():
-            c_left(z, j, u, n)
-
-    def own_chunks(j, carry):
-        at(j, own_chunk)
+            c_left(z, j)
+
         return carry
 
     lax.fori_loop(0, nj, own_chunks, 0)
@@ -332,35 +330,35 @@
             fn(z + d)
 
     def ahead(t):
-        def one(d, j, u, n):
+        def one(d, j):
             @pl.when(z == 1)
             def _():
                 if d == 0:
-                    c_right(z, j, u, n)
+                    c_right(z, j)
                 elif d == 1:
-                    arrive(z - 1, j, u, n)
-                    c_right(z - 1, j, u, n)
-                    arrive(z + 1, j, u, n)
+                    arrive(z - 1, j)
+                    c_right(z - 1, j)
+                    arrive(z + 1, j)
                 else:
-                    arrive(z + 2, j, u, n)
+                    arrive(z + 2, j)
                     for src in range(nz - 1):
-                        c_left(z + src, j, u, n)
+                        c_left(z + src, j)
 
             @pl.when(z == 2)
             def _():
                 if d == 0:
-                    c_left(z, j, u, n)
+                    c_left(z, j)
                 elif d == 1:
-                    arrive(z + 1, j, u, n)
-                    c_left(z + 1, j, u, n)
-                    arrive(z - 1, j, u, n)
+                    arrive(z + 1, j)
+                    c_left(z + 1, j)
+                    arrive(z - 1, j)
                 else:
-                    arrive(z - 2, j, u, n)
+                    arrive(z - 2, j)
                     for src in range(nz - 1):
-                        c_right(z - src, j, u, n)
+                        c_right(z - src, j)
 
         for d in range(nz - 1):
-            at(t + nz - 1 - d, functools.partial(one, d))
+            at(t + LOOK * (nz - 1 - d), functools.partial(one, d))
 
     for p in range(2):
         with jax.named_scope(f"forward1_{p}"):
@@ -378,7 +376,8 @@
         for p in range(2):
             with jax.named_scope(f"forward{d}_{p}"):
                 forward(d, p)
-    ahead(1 - nz)
+    for t in range(LOOK):
+        ahead(t - LOOK * (nz - 1))
     with jax.named_scope("gate_wait"):
         for k in range(ne - 1):
             await_gate(k)
@@ -395,7 +394,8 @@
         with jax.named_scope(f"hidden{d}"):
             both(d, hidden)
         with jax.named_scope(f"ahead{d}"):
-            ahead(d + 1 - nz)
+            for t in range(LOOK):
+                ahead(t - LOOK * (nz - 1 - d))
     with jax.named_scope("dense_wait"):
         for p in range(3):
             for k in range(ne - 1):
@@ -416,103 +416,89 @@
     with jax.named_scope("up_last"):
         both(nz - 1, functools.partial(up_part, far=True))
 
-    def back(k, j, u, n):
+    def back(k, j):
         block = (diagonal, diagonal, across, along, along, across)[k]
         peer = (across, along, across, along, along, across)[k]
         spot = (0, 1, 0, 1, 1, 0)[k]
-        to = pl.ds(u, n)
-        lands = relay.at[k, to] if k < 2 else yrecv.at[spot, k % 2, to]
-        piece = ysend.at[block, k % 2, to]
-        return remote(piece, lands, rsend.at[0], rrecv.at[j, min(k, 2)], ep=peer)
-
-    def await_back(j, u, n):
-        piece = yrecv.at[:, :, pl.ds(u, n)]
-        remote(piece, piece, rsend.at[0], rrecv.at[j, 2], ep=across).wait_recv()
-
-    def take(j, u, n):
+        lands = relay.at[k, j] if k < 2 else yrecv.at[spot, k % 2, j]
+        return remote(ysend.at[block, k % 2, j], lands, rsend.at[0], rrecv.at[j, min(k // 2, 1)], ep=peer)
+
+    def take(j):
         ahead(j)
 
         @pl.when(z == 0)
         def _():
             for d in range(1, nz):
-                arrive(d, j, u, n)
+                arrive(d, j)
 
         @pl.when(z == nz - 1)
         def _():
             for d in range(1, nz):
-                arrive(z - d, j, u, n)
-
-        piece = ws.at[:, 1 - c, 2, columns(u, n)]
+                arrive(z - d, j)
+
+        piece = ws.at[:, 1 - c, 2, columns(j)]
         remote(piece, piece, wpartner.at[0], precv.at[j], tp=partner).wait_recv()
 
-    def produce(j, u, n):
-        here = columns(u, n)
+    def produce(j):
+        here = columns(j)
         w = jnp.concatenate([ws[s, i, 2, here, :] for s in range(nz) for i in range(CORES)], axis=1)
-
-        def rows_of(b):
-            return lax.dot_general(
-                hbuf[b], w, (((1,), (1,)), ((), ())), preferred_element_type=jnp.float32
-            )
-
-        def put(y, *lead):
-            ref, lead = lead[0], lead[1:]
-            for i in range(n):
-                ref[lead + (u + i,)] = y[:, i * UNIT : (i + 1) * UNIT].astype(ref.dtype)
-
-        y = rows_of(diagonal)
-        for k in range(2):
-            put(y[k * half : (k + 1) * half], ysend, diagonal, k)
-            back(k, j, u, n).start()
-        y = rows_of(across)
-        put(y[:half], ysend, across, 0)
-        put(y[half:], keep, 1)
-        back(2, j, u, n).start()
-        y = rows_of(along)
-        put(y[half:], ysend, along, 1)
-        put(y[:half], keep, 0)
-        back(3, j, u, n).start()
-        own[:, here] = rows_of(me)
-
-    def pass_on(j, u, n):
+        blocks = (diagonal, across, along, me)
+        full = lax.dot_general(
+            jnp.concatenate([hbuf[b] for b in blocks], axis=0), w,
+            (((1,), (1,)), ((), ())), preferred_element_type=jnp.float32,
+        )
+        y = [full[i * half : (i + 1) * half] for i in range(2 * ne)]
+        for k, i in enumerate((0, 1, 2, 5)):
+            ysend[blocks[i // 2], i % 2, j] = y[i].astype(jnp.bfloat16)
+            back(k, j).start()
+        keep[0, j] = y[4]
+        keep[1, j] = y[3]
+        own[:, here] = full[(ne - 1) * rows :]
+
+    def pass_on(j):
+        piece = relay.at[:, j]
+        remote(piece, piece, rsend.at[0], rrecv.at[j, 0], ep=across).wait_recv()
         for k, block in enumerate((along, across)):
-            back(k, j, u, n).wait_recv()
-            for i in range(n):
-                v = keep[k, u + i] + relay[k, u + i].astype(jnp.float32)
-                ysend[block, k, u + i] = v.astype(jnp.bfloat16)
-            back(4 + k, j, u, n).start()
-
-    def combine(j, u, n):
-        await_back(j, u, n)
-        for i in range(n):
-            here = columns(u + i, 1)
-            for h in range(2):
-                low = h * half
-                total = side[low : low + half, here] + own[low : low + half, here]
-                for k in range(2):
-                    total = total + yrecv[k, h, u + i].astype(jnp.float32)
-                out_ref[low : low + half, here] = total.astype(jnp.bfloat16)
-
-    def scoped(name, j, fn):
-        with jax.named_scope(name):
-            at(j, fn)
+            v = keep[k, j] + relay[k, j].astype(jnp.float32)
+            ysend[block, k, j] = v.astype(jnp.bfloat16)
+            back(4 + k, j).start()
+
+    def combine(j):
+        piece = yrecv.at[:, :, j]
+        remote(piece, piece, rsend.at[0], rrecv.at[j, 1], ep=across).wait_recv()
+        here = columns(j)
+        for h in range(2):
+            low = h * half
+            total = side[low : low + half, here] + own[low : low + half, here]
+            for k in range(2):
+                total = total + yrecv[k, h, j].astype(jnp.float32)
+            out_ref[low : low + half, here] = total.astype(jnp.bfloat16)
 
     def step(j, carry):
-        take(j, 2 * j - 1, 2)
+        with jax.named_scope("take"):
+            take(j)
         with jax.named_scope("produce"):
-            produce(j, 2 * j - 1, 2)
-        scoped("pass_on", j - 1, pass_on)
-        scoped("combine", j - 2, combine)
+            produce(j)
+        with jax.named_scope("pass_on"):
+            at(j - BEHIND, pass_on)
+        with jax.named_scope("combine"):
+            pl.when(j < nj - 2)(lambda: at(j - 2 * BEHIND, combine))
         return carry
 
-    scoped("take", 0, take)
-    scoped("produce", 0, produce)
-    lax.fori_loop(1, nj - 1, step, 0)
-    scoped("take", nj - 1, take)
-    scoped("produce", nj - 1, produce)
-    scoped("pass_on", nj - 2, pass_on)
-    scoped("pass_on", nj - 1, pass_on)
-    for j in range(nj - 3, nj):
-        scoped("combine", j, combine)
+    lax.fori_loop(0, nj, step, 0)
+
+    def pass_rest(j, carry):
+        pass_on(j)
+        return carry
+
+    def combine_rest(j, carry):
+        combine(j)
+        return carry
+
+    with jax.named_scope("pass_rest"):
+        lax.fori_loop(nj - BEHIND, nj, pass_rest, 0)
+    with jax.named_scope("combine_rest"):
+        lax.fori_loop(nj - 2 * BEHIND - 2, nj, combine_rest, 0)
 
     drain = jax.named_scope("drain")
     drain.__enter__()
@@ -563,8 +549,7 @@
     rows, width = tokens.shape
     topk = expert_ids.shape[1]
     shard = w_gate.shape[2]
-    units = width // UNIT
-    nj = units // 2 + 1
+    nj = width // UNIT
     half = rows // 2
     bf, f32 = jnp.bfloat16, jnp.float32
     dma = pltpu.SemaphoreType.DMA
@@ -586,10 +571,10 @@
             pltpu.VMEM((ne, rows, CORES * shard), f32),
             pltpu.VMEM((ne, rows, tp * shard), bf),
             pltpu.VMEM((rows, width), f32),
-            pltpu.VMEM((2, units, half, UNIT), f32),
-            pltpu.VMEM((ne, 2, units, half, UNIT), bf),
-            pltpu.VMEM((2, 2, units, half, UNIT), bf),
-            pltpu.VMEM((2, units, half, UNIT), bf),
+            pltpu.VMEM((2, nj, half, UNIT), f32),
+            pltpu.VMEM((ne, 2, nj, half, UNIT), bf),
+            pltpu.VMEM((2, 2, nj, half, UNIT), bf),
+            pltpu.VMEM((2, nj, half, UNIT), bf),
             pltpu.VMEM((rows, width), f32),
             pltpu.VMEM((rows, 1), f32),
             pltpu.VMEM((ne, SUB, rows), f32),
@@ -605,7 +590,7 @@
             dma((nz,)),
             dma((2,)),
             dma((1,)),
-            dma((nj, nz)),
+            dma((nj, nz - 1)),
             dma((nj,)),
             dma((4,)),
             dma((4,)),
@@ -613,7 +598,7 @@
             dma((6,)),
             dma((2 * ne - 2, 3)),
             dma((1,)),
-            dma((nj, 3)),
+            dma((nj, 2)),
         ],
         compiler_params=pltpu.CompilerParams(
             collective_id=0, has_side_effects=True, vmem_limit_bytes=VMEM_BYTES
@@ -634,7 +619,7 @@
     size = 2 * ne * block * 2 + 24 * block + 6 * width * shard * tp
     size += 2 * ne * rows * shard * tp + 6 * ne * dense_gate.size + 1024 * ne * rows
     size += 8 * ne * rows * shard
-    aligned = shard % 128 == 0 and width % (2 * UNIT) == 0 and width > TAIL and rows % 64 == 0
+    aligned = shard % 128 == 0 and width % (8 * UNIT) == 0 and width > TAIL and rows % 64 == 0
     return ne == 4 and tp == 4 * CORES and aligned and size < VMEM_BYTES * 15 // 16
 
 

time: 119 us -> 118 us (level)
    pallas_call x1, Pallas kernels: 118 us -> 117 us  [fused_layer(): pl.pallas_call(functools.partial(moe_kernel, ne, nz), out_shape=pltpu.VME...]
where the time goes in v5:
time: 118 us
  Pallas kernels  117 us (99%)
    pallas_call x1, Pallas kernels, fused_layer(): pl.pallas_call(functools.partial(moe_kernel, ne, nz), out_shape=pltpu.VME...  117 us

profile of v5, /device:TPU:0, one launch (start us, length us, event | category | flops | bytes accessed | tf_op | source)
XLA Modules:
  0.0 117.9 jit_solution(3215025616515115773)
XLA Ops:
  0.0 116.9 %shard_map.109 = bf16[256,2048]{1,0:T(8,128)(2,1)S(1)} custom-call(bf16[256,2048]{1,0:T(8,128)(2,1)} %x_hbm.1, bf16[2048,128]{1,0:T(8,128)(2,1)} %bitcast.7, bf16[2048,128]{1,0:T(8,128)(2,1)} %bitcast.8, bf16[2048,128]{1,0:T(8,128)(2,1)} %bitcast.9, bf16[512,256]{1,0:T(8,128)(2,1)} %dg_hbm.1, bf16[512,256]{1,0:T(8,128)(2,1)} %du_hbm.1, ...), custom_call_target="tpu_custom_call" | custom-call | flops 12884901888 | bytes 4194304 | tf_op jit(solution)/shard_map/pallas_call | solution.py:559
  116.9 1.0 copy.13

commit v6 on v5

--- a/solution.py
+++ b/solution.py
@@ -140,13 +140,13 @@
         peer = (across, along, along, across)[k]
         low, size = ((0, rows), (0, rows), (0, half), (half, half))[k]
         piece = xg.at[block, low : low + size]
-        return remote(piece, piece, tsend.at[k], trecv.at[k], ep=peer)
+        return remote(piece, piece, tsend.at[0], trecv.at[k], ep=peer)
 
     def await_token(k):
         block = (across, along, diagonal, diagonal)[k]
         low, size = ((0, rows), (0, rows), (0, half), (half, half))[k]
         piece = xg.at[block, low : low + size]
-        remote(piece, piece, tsend.at[k], trecv.at[k], ep=across).wait_recv()
+        remote(piece, piece, tsend.at[0], trecv.at[k], ep=across).wait_recv()
 
     def gate_copy(k):
         return remote(wts.at[0], wts.at[1 + k], gsem.at[0], gsem.at[1 + k], ep=peers[k])
@@ -166,16 +166,15 @@
 
     def dense_copy(k, p):
         lands = dense_piece(p, 1 + k, c)
-        return remote(dense_piece(p, 0, c), lands, dsem.at[p], drecv.at[k, p], ep=peers[k])
-
-    def dense_partner(k, p, color):
-        piece = dense_piece(p, 1 + k, color)
-        return remote(piece, piece, dsem.at[3 + p], drecv.at[ne - 1 + k, p], tp=partner)
-
-    def dense_sent(p):
-        piece = dense_piece(p, pl.ds(1, ne - 1), c)
-        for first in (0, 3):
-            remote(piece, piece, dsem.at[first + p], drecv.at[0, p], tp=partner).wait_send()
+        return remote(dense_piece(p, 0, c), lands, dsem.at[p], drecv.at[0, p], ep=peers[k])
+
+    def dense_partner(k, p):
+        piece = dense_piece(p, 1 + k, c)
+        return remote(piece, piece, dsem.at[3 + p], drecv.at[1, p], tp=partner)
+
+    def dense_all(p, i, color):
+        piece = dense_piece(p, pl.ds(1, ne - 1), color)
+        return remote(piece, piece, dsem.at[3 * i + p], drecv.at[i, p], tp=partner)
 
     for p in range(2):
         local[p].wait()
@@ -398,17 +397,16 @@
                 ahead(t - LOOK * (nz - 1 - d))
     with jax.named_scope("dense_wait"):
         for p in range(3):
+            dense_all(p, 0, c).wait_recv()
             for k in range(ne - 1):
-                dense_copy(k, p).wait_recv()
-                dense_partner(k, p, c).start()
+                dense_partner(k, p).start()
     with jax.named_scope("forward_last0"):
         forward(nz - 1, 0)
     with jax.named_scope("gate_last"):
         both(nz - 1, gate_part)
     with jax.named_scope("dense_partner"):
         for p in range(3):
-            for k in range(ne - 1):
-                dense_partner(k, p, 1 - c).wait_recv()
+            dense_all(p, 1, 1 - c).wait_recv()
     with jax.named_scope("dense_side"):
         dense_side([me] + peers, me, xg, dgs, dus, dds, mix_ref, side)
     with jax.named_scope("forward_last1"):
@@ -477,10 +475,10 @@
     def step(j, carry):
         with jax.named_scope("take"):
             take(j)
+        with jax.named_scope("pass_on"):
+            pl.when(j < nj - 1)(lambda: at(j - BEHIND, pass_on))
         with jax.named_scope("produce"):
             produce(j)
-        with jax.named_scope("pass_on"):
-            at(j - BEHIND, pass_on)
         with jax.named_scope("combine"):
             pl.when(j < nj - 2)(lambda: at(j - 2 * BEHIND, combine))
         return carry
@@ -496,17 +494,18 @@
         return carry
 
     with jax.named_scope("pass_rest"):
-        lax.fori_loop(nj - BEHIND, nj, pass_rest, 0)
+        lax.fori_loop(nj - 1 - BEHIND, nj, pass_rest, 0)
     with jax.named_scope("combine_rest"):
         lax.fori_loop(nj - 2 * BEHIND - 2, nj, combine_rest, 0)
 
     drain = jax.named_scope("drain")
     drain.__enter__()
-    for k in range(4):
-        token_copy(k).wait_send()
+    piece = xg.at[: ne - 1]
+    remote(piece, piece, tsend.at[0], trecv.at[0], ep=across).wait_send()
     gate_all().wait_send()
     for p in range(3):
-        dense_sent(p)
+        for i in range(2):
+            dense_all(p, i, c).wait_send()
     for src in range(nz):
         for sems, there, far in (
             (wright, (z < nz - 1) & (z >= src), (z == nz - 2) & (src == 0)),
@@ -592,11 +591,11 @@
             dma((1,)),
             dma((nj, nz - 1)),
             dma((nj,)),
-            dma((4,)),
+            dma((1,)),
             dma((4,)),
             dma((ne,)),
             dma((6,)),
-            dma((2 * ne - 2, 3)),
+            dma((2, 3)),
             dma((1,)),
             dma((nj, 2)),
         ],

time: 118 us -> 117 us (level)
  no operation moved by 1% of the time
where the time goes in v6:
time: 117 us
  Pallas kernels  116 us (99%)
    pallas_call x1, Pallas kernels, fused_layer(): pl.pallas_call(functools.partial(moe_kernel, ne, nz), out_shape=pltpu.VME...  116 us

profile of v6, /device:TPU:0, one launch (start us, length us, event | category | flops | bytes accessed | tf_op | source)
XLA Modules:
  0.0 117.3 jit_solution(9800597408483236046)
XLA Ops:
  0.0 116.4 %shard_map.109 = bf16[256,2048]{1,0:T(8,128)(2,1)S(1)} custom-call(bf16[256,2048]{1,0:T(8,128)(2,1)} %x_hbm.1, bf16[2048,128]{1,0:T(8,128)(2,1)} %bitcast.7, bf16[2048,128]{1,0:T(8,128)(2,1)} %bitcast.8, bf16[2048,128]{1,0:T(8,128)(2,1)} %bitcast.9, bf16[512,256]{1,0:T(8,128)(2,1)} %dg_hbm.1, bf16[512,256]{1,0:T(8,128)(2,1)} %du_hbm.1, ...), custom_call_target="tpu_custom_call" | custom-call | flops 12884901888 | bytes 4194304 | tf_op jit(solution)/shard_map/pallas_call | solution.py:558
  116.4 1.0 copy.13

commit v7 on v6

--- a/solution.py
+++ b/solution.py
@@ -38,6 +38,19 @@
     peers = [across, along, diagonal]
     partner = z * CORES + (1 - c)
 
+    barrier = pltpu.get_barrier_semaphore()
+    for peer in (across, along):
+        pl.semaphore_signal(barrier, inc=1, device_id={"ep": peer}, device_id_type=MESH)
+    pl.semaphore_signal(barrier, inc=1, device_id={"tp": partner}, device_id_type=MESH)
+
+    @pl.when(z > 0)
+    def _():
+        pl.semaphore_signal(barrier, inc=1, device_id={"tp": tp - CORES}, device_id_type=MESH)
+
+    @pl.when(z < nz - 1)
+    def _():
+        pl.semaphore_signal(barrier, inc=1, device_id={"tp": tp + CORES}, device_id_type=MESH)
+
     local = [pltpu.make_async_copy(wg_hbm, ws.at[z, c, 0], lsem.at[0])]
     local.append(pltpu.make_async_copy(wu_hbm, ws.at[z, c, 1], lsem.at[1]))
     local.append(pltpu.make_async_copy(x_hbm, xin, lsem.at[2]))
@@ -49,19 +62,6 @@
         local.append(pltpu.make_async_copy(ref, slot, lsem.at[7 + p]))
     for copy in local:
         copy.start()
-
-    barrier = pltpu.get_barrier_semaphore()
-    for peer in (across, along):
-        pl.semaphore_signal(barrier, inc=1, device_id={"ep": peer}, device_id_type=MESH)
-    pl.semaphore_signal(barrier, inc=1, device_id={"tp": partner}, device_id_type=MESH)
-
-    @pl.when(z > 0)
-    def _():
-        pl.semaphore_signal(barrier, inc=1, device_id={"tp": tp - CORES}, device_id_type=MESH)
-
-    @pl.when(z < nz - 1)
-    def _():
-        pl.semaphore_signal(barrier, inc=1, device_id={"tp": tp + CORES}, device_id_type=MESH)
 
     neighbours = (z + nz - 1) // nz + (2 * nz - 2 - z) // nz
     with jax.named_scope("barrier"):

time: 117 us -> 117 us (level)
  no operation moved by 1% of the time
where the time goes in v7:
time: 117 us
  Pallas kernels  116 us (99%)
    pallas_call x1, Pallas kernels, fused_layer(): pl.pallas_call(functools.partial(moe_kernel, ne, nz), out_shape=pltpu.VME...  116 us

profile of v7, /device:TPU:0, one launch (start us, length us, event | category | flops | bytes accessed | tf_op | source)
XLA Modules:
  0.0 117.3 jit_solution(15362692611269792670)
XLA Ops:
  0.0 116.3 %shard_map.109 = bf16[256,2048]{1,0:T(8,128)(2,1)S(1)} custom-call(bf16[256,2048]{1,0:T(8,128)(2,1)} %x_hbm.1, bf16[2048,128]{1,0:T(8,128)(2,1)} %bitcast.7, bf16[2048,128]{1,0:T(8,128)(2,1)} %bitcast.8, bf16[2048,128]{1,0:T(8,128)(2,1)} %bitcast.9, bf16[512,256]{1,0:T(8,128)(2,1)} %dg_hbm.1, bf16[512,256]{1,0:T(8,128)(2,1)} %du_hbm.1, ...), custom_call_target="tpu_custom_call" | custom-call | flops 12884901888 | bytes 4194304 | tf_op jit(solution)/shard_map/pallas_call | solution.py:558
  116.3 1.0 copy.13
